TPU v7x, 32 devices: a whole 2x2x4 slice. The times are simulated.
32 devices in a mesh: ep: 8 (over z, y), tp: 4 (over x, core).
Axes of the slice: x: 2, y: 2, z: 4, core: 2. Of those that a mesh axis runs over, the one named last changes fastest.
Arguments:
- query_rows: bfloat16 [4096, 2048], P('ep', 'tp'), may hold values from -6 to 6
- key_rows: bfloat16 [4096, 512], P('ep', 'tp'), may hold values from -6 to 6
- value_rows: bfloat16 [4096, 512], P('ep', 'tp'), may hold values from -6 to 6
- query_gain: float32 [64], replicated, may hold values from 0.2 to 4.5
- key_gain: float32 [64], replicated, may hold values from 0.2 to 4.5
- sink_logit: float32 [32], P('tp'), may hold values from 2 to 6
- out_weight: bfloat16 [2048, 2048], P('tp'), may hold values from -0.125 to 0.125
- tokens: bfloat16 [4096, 2048], P('ep'), may hold values from -6 to 6
- norm_gain: float32 [2048], replicated, may hold values from 0.1 to 1.9
- expert_ids: int32 [4096, 2], P('ep'), may hold values from 0 to 31, all different within a row; in each aligned block of 128 rows (0 to 127, 128 to 255, ...) at most 16 rows name the same one
- route_weight: float32 [4096, 2], P('ep'), may hold values from 0.2 to 1
- gate_weight: bfloat16 [32, 2048, 1024], P('ep', None, 'tp'), may hold values from -0.125 to 0.125
- up_weight: bfloat16 [32, 2048, 1024], P('ep', None, 'tp'), may hold values from -0.125 to 0.125
- down_weight: bfloat16 [32, 1024, 2048], P('ep', 'tp'), may hold values from -0.1875 to 0.1875
- shared_gate: bfloat16 [2048, 1024], P(None, 'tp'), may hold values from -0.125 to 0.125
- shared_up: bfloat16 [2048, 1024], P(None, 'tp'), may hold values from -0.125 to 0.125
- shared_down: bfloat16 [1024, 2048], P('tp'), may hold values from -0.1875 to 0.1875
Outputs:
- mixer_out: bfloat16 [4096, 2048], P(('ep', 'tp'))
- expert_out: bfloat16 [4096, 2048], P(('ep', 'tp'))
Inputs may be any that keep to these rules, and one draw needn't show every extreme that they name: `expert_ids`: each row names 2 different experts. In each aligned block of 128 rows no expert is named by more than 16 rows, a bound that some block reaches.
All inputs are finite; a program needn't handle non-finite values.
Results may differ from a plain program's by a relative error of at most 0.012.
The roundings to bfloat16 on the way count: a program that leaves them out, or rounds other values in their place, can miss the bound.
Values may be sent and summed in bfloat16 or wider, within the bound.
A program may use at most 128 MiB of HBM per device.

v0:
```python
import functools
import jax
import jax.numpy as jnp
from jax import lax
from jax.experimental import pallas as pl
from jax.experimental.pallas import tpu as pltpu
from jax.sharding import PartitionSpec as P

HEADS = 32
KV_HEADS = 8
HEAD_DIM = 64
WINDOW = 128
BLOCK = 128
TOP_K = 2


epsilon = 1e-06
masked_score = -1e30
score_scale = 0.125


def from_behind(block, axis, distance):
    devices = range(lax.axis_size(axis))
    route = [(i - distance, i) for i in devices if i - distance in devices]
    return lax.ppermute(block, axis, route)


def rms_scale(values, gain):
    widened = values.astype(jnp.float32)
    scaled = widened * lax.rsqrt(jnp.mean(widened * widened, axis=-1, keepdims=True) + epsilon)
    return (scaled * gain).astype(jnp.bfloat16)


def window_mask(first_block, block_count):
    query_pos = jnp.arange(BLOCK)[:, None]
    key_pos = jnp.arange(2 * BLOCK)[None, :]
    inside = (key_pos <= query_pos + BLOCK) & (key_pos > query_pos + BLOCK - WINDOW)
    not_first = (first_block + jnp.arange(block_count))[:, None, None] > 0
    return inside[None] & (not_first | (key_pos[None] >= BLOCK))


def band_blocks(rim_block, blocks_in):
    joined = jnp.concatenate([rim_block[None], blocks_in], axis=0)
    return jnp.concatenate([joined[:-1], joined[1:]], axis=1)


def attention_part(query_rows, key_rows, value_rows, query_gain, key_gain, sink_logit):
    sequence_rows = query_rows.shape[0]
    blocks = sequence_rows // BLOCK
    pair_heads = key_rows.shape[1] // HEAD_DIM
    group_size = HEADS // KV_HEADS
    query_normed = rms_scale(
        query_rows.reshape(blocks, BLOCK, pair_heads, group_size, HEAD_DIM), query_gain
    )
    key_normed = rms_scale(key_rows.reshape(blocks, BLOCK, pair_heads, HEAD_DIM), key_gain)
    value_blocks = value_rows.reshape(blocks, BLOCK, pair_heads, HEAD_DIM)
    rim_keys, rim_values = from_behind((key_normed[blocks - 1], value_blocks[blocks - 1]), "ep", 1)
    key_band = band_blocks(rim_keys, key_normed)
    value_band = band_blocks(rim_values, value_blocks)
    window = window_mask(lax.axis_index("ep") * blocks, blocks)
    scores = (
        jnp.einsum("nqhgd,nkhd->hgnqk", query_normed, key_band, preferred_element_type=jnp.float32)
        * score_scale
    )
    scores = jnp.where(window[None, None], scores, masked_score)
    sink_col = sink_logit.reshape(pair_heads, group_size, 1, 1, 1)
    row_max = jnp.maximum(jnp.max(scores, axis=-1, keepdims=True), sink_col)
    exp_scores = jnp.exp(scores - row_max)
    attn_probs = (
        exp_scores / (jnp.sum(exp_scores, axis=-1, keepdims=True) + jnp.exp(sink_col - row_max))
    ).astype(jnp.bfloat16)
    heads_out = (
        jnp.einsum("hgnqk,nkhd->nqhgd", attn_probs, value_band, preferred_element_type=jnp.float32)
        .astype(jnp.bfloat16)
        .reshape(sequence_rows, pair_heads * group_size * HEAD_DIM)
    )
    return heads_out


def exchange_kernel(
    ranks,
    group,
    local_experts,
    capacity,
    outgoing,
    outgoing_peer,
    mixer_part,
    shared_part,
    gate_hbm,
    up_hbm,
    down_hbm,
    returned,
    mixer_sum,
    shared_sum,
    rows,
    kept,
    sibling_send,
    sibling_recv,
    peer_send,
    peer_recv,
    finished,
    early_recv,
    early_send,
    early_peer,
    out_sems,
    in_sems,
    fan_send,
    fan_recv,
    add_send,
    add_recv,
    back_send,
    back_recv,
    early_s,
    early_r,
    own_sem,
    gate,
    up,
    down,
    weight_sem,
):
    rank = lax.axis_index("ep")
    part = lax.axis_index("tp")
    sibling = part + 1 - 2 * lax.rem(part, 2)
    peer = lax.rem(part + 2, 4)
    across = 3 - part
    f32, bf16 = jnp.float32, jnp.bfloat16
    mesh_ids = pl.DeviceIdType.MESH

    def partner(k, sign=1):
        half = ranks // 2
        return lax.rem(rank // 2 + half + sign * (k // 2), half) * 2 + lax.rem(
            lax.rem(rank, 2) + k, 2
        )

    def send(source, target, send_sem, recv_sem, ep_to, tp_to):
        copy = pltpu.make_async_remote_copy(
            src_ref=source,
            dst_ref=target,
            send_sem=send_sem,
            recv_sem=recv_sem,
            device_id=(ep_to, tp_to),
            device_id_type=mesh_ids,
        )
        copy.start()
        return copy

    barrier = pltpu.get_barrier_semaphore()
    for k in range(1, ranks):
        pl.semaphore_signal(
            barrier, inc=1, device_id=(partner(k), part), device_id_type=mesh_ids
        )
    for other in (sibling, peer):
        pl.semaphore_signal(barrier, inc=1, device_id=(rank, other), device_id_type=mesh_ids)
    pl.semaphore_wait(barrier, ranks + 1)

    own = pltpu.make_async_copy(outgoing.at[0], rows.at[0, 0], own_sem)
    own.start()
    to_sibling = {}
    to_peer = {}
    to_peer[1] = send(
        outgoing_peer.at[1], rows.at[1, 2], fan_send.at[0, 1], fan_recv.at[0, 1], partner(1), part
    )
    beside = pltpu.make_async_copy(outgoing_peer.at[0], rows.at[0, 2], fan_recv.at[0, 0])
    beside.start()
    dispatched = [None] + [
        send(
            outgoing.at[k],
            rows.at[k, 0],
            out_sems.at[k],
            in_sems.at[k],
            partner(k),
            part,
        )
        for k in range(1, ranks)
    ]
    early = []
    for i, full in enumerate((mixer_part, shared_part)):
        for j, which in enumerate((across, sibling)):
            s = 2 * i + j
            early.append(
                send(
                    full.at[which],
                    early_recv.at[s],
                    early_s.at[s],
                    early_r.at[s],
                    rank,
                    sibling,
                )
            )
    loads = [
        pltpu.make_async_copy(source, held, weight_sem.at[i])
        for i, (source, held) in enumerate(((gate_hbm, gate), (up_hbm, up), (down_hbm, down)))
    ]
    for load in loads:
        load.start()
    relayed = {}
    added = {}
    peered = {}
    backs = {}

    def fan_out(k):
        if k == 0:
            own.wait()
        else:
            dispatched[k].wait_recv()
        if k > 1:
            to_peer[k] = send(
                rows.at[k, 0], rows.at[k, 2], fan_send.at[0, k], fan_recv.at[0, k], rank, peer
            )
        to_sibling[k] = send(
            rows.at[k, 0], rows.at[k, 1], fan_send.at[1, k], fan_recv.at[1, k], rank, sibling
        )

    def relay(k):
        if k == 0:
            beside.wait()
        else:
            to_peer[k].wait_recv()
        relayed[k] = send(
            rows.at[k, 2], rows.at[k, 3], fan_send.at[2, k], fan_recv.at[2, k], rank, sibling
        )

    def early_add():
        for i, full in enumerate((mixer_part, shared_part)):
            early[2 * i].wait_recv()
            early_send[i] = (
                full[peer].astype(f32) + early_recv[2 * i].astype(f32)
            ).astype(bf16)
            early.append(
                send(
                    early_send.at[i],
                    early_peer.at[i],
                    early_s.at[4 + i],
                    early_r.at[4 + i],
                    rank,
                    peer,
                )
            )

    def early_finish():
        for i, (full, total) in enumerate(((mixer_part, mixer_sum), (shared_part, shared_sum))):
            early[2 * i + 1].wait_recv()
            early[4 + i].wait_recv()
            total[...] = (
                full[part].astype(f32)
                + early_recv[2 * i + 1].astype(f32)
                + early_peer[i].astype(f32)
            ).astype(bf16)

    def experts(g):
        first = g * group
        for k in range(first, first + group):
            to_sibling[k].wait_recv()
            relayed[k].wait_recv()
        if g == 0:
            for load in loads:
                load.wait()
        width = rows.shape[-1]

        def one(index, carry):
            at = pl.ds(pl.multiple_of(index * capacity, capacity), capacity)
            block = rows[first : first + group, :, at, :].reshape(group * 4 * capacity, width)
            gate_part = jnp.dot(block, gate[index], preferred_element_type=f32)
            up_part = jnp.dot(block, up[index], preferred_element_type=f32)
            hidden = (gate_part / (1.0 + jnp.exp(-gate_part)) * up_part).astype(bf16)
            made = jnp.dot(hidden, down[index], preferred_element_type=f32)
            made = made.astype(bf16).reshape(group, 4, capacity, width)
            spot = pl.ds(first, group)
            kept[spot, 0, at, :] = made[:, 0]
            sibling_send[spot, 0, at, :] = made[:, 1]
            kept[spot, 1, at, :] = made[:, 2]
            sibling_send[spot, 1, at, :] = made[:, 3]
            return carry

        lax.fori_loop(0, local_experts, one, 0)
        for k in range(first, first + group):
            added[k] = send(
                sibling_send.at[k],
                sibling_recv.at[k],
                add_send.at[0, k],
                add_recv.at[0, k],
                rank,
                sibling,
            )

    def pair_add(k):
        added[k].wait_recv()
        peer_send[k] = (kept[k, 1].astype(f32) + sibling_recv[k, 1].astype(f32)).astype(bf16)
        peered[k] = send(
            peer_send.at[k], peer_recv.at[k], add_send.at[1, k], add_recv.at[1, k], rank, peer
        )

    def finish(k):
        peered[k].wait_recv()
        total = (
            kept[k, 0].astype(f32) + sibling_recv[k, 0].astype(f32) + peer_recv[k].astype(f32)
        ).astype(bf16)
        if k == 0:
            returned[0] = total
        else:
            finished[k] = total
            backs[k] = send(
                finished.at[k],
                returned.at[k],
                back_send.at[k],
                back_recv.at[k],
                partner(k, -1),
                part,
            )

    groups = ranks // group
    for step in range(groups + 4):
        for stage, work in ((0, fan_out), (1, relay)):
            g = step - stage
            if 0 <= g < groups:
                for k in range(g * group, (g + 1) * group):
                    work(k)
        if step == 0:
            early_add()
        if 0 <= step - 3 < groups:
            for k in range((step - 3) * group, (step - 2) * group):
                pair_add(k)
        if 0 <= step - 2 < groups:
            experts(step - 2)
        if 0 <= step - 4 < groups:
            for k in range((step - 4) * group, (step - 3) * group):
                finish(k)
        if step == 2:
            early_finish()
    for k in range(1, ranks):
        backs[k].wait_recv()
    for k in range(1, ranks):
        dispatched[k].wait_send()
        backs[k].wait_send()
    for table in (to_peer, to_sibling, relayed, added, peered):
        for k in table:
            table[k].wait_send()
    for copy in early:
        copy.wait_send()


def exchange(outgoing, outgoing_peer, mixer_part, shared_part, gate, up, down, capacity):
    ranks, share, width = outgoing.shape
    quarter = mixer_part.shape[1]
    local_experts = gate.shape[0]
    group = 1
    bf16 = jnp.bfloat16
    dma = pltpu.SemaphoreType.DMA
    vmem = pl.BlockSpec(memory_space=pltpu.VMEM)
    return pl.pallas_call(
        functools.partial(exchange_kernel, ranks, group, local_experts, capacity),
        out_shape=(
            jax.ShapeDtypeStruct((ranks, share, width), bf16),
            jax.ShapeDtypeStruct((quarter, width), bf16),
            jax.ShapeDtypeStruct((quarter, width), bf16),
        ),
        in_specs=[vmem] * 4 + [pl.BlockSpec(memory_space=pl.ANY)] * 3,
        out_specs=(vmem,) * 3,
        scratch_shapes=[
            pltpu.VMEM((ranks, 4, share, width), bf16),
            pltpu.VMEM((ranks, 2, share, width), bf16),
            pltpu.VMEM((ranks, 2, share, width), bf16),
            pltpu.VMEM((ranks, 2, share, width), bf16),
            pltpu.VMEM((ranks, share, width), bf16),
            pltpu.VMEM((ranks, share, width), bf16),
            pltpu.VMEM((ranks, share, width), bf16),
            pltpu.VMEM((4, quarter, width), bf16),
            pltpu.VMEM((2, quarter, width), bf16),
            pltpu.VMEM((2, quarter, width), bf16),
            dma((ranks,)),
            dma((ranks,)),
            dma((3, ranks)),
            dma((3, ranks)),
            dma((2, ranks)),
            dma((2, ranks)),
            dma((ranks,)),
            dma((ranks,)),
            dma((6,)),
            dma((6,)),
            dma,
            pltpu.VMEM(gate.shape, bf16),
            pltpu.VMEM(up.shape, bf16),
            pltpu.VMEM(down.shape, bf16),
            dma((3,)),
        ],
        compiler_params=pltpu.CompilerParams(
            collective_id=0, has_side_effects=True, vmem_limit_bytes=64000 * 1024
        ),
    )(outgoing, outgoing_peer, mixer_part, shared_part, gate, up, down)


def wide_shards(
    query_rows,
    key_rows,
    value_rows,
    query_gain,
    key_gain,
    sink_logit,
    out_weight,
    tokens,
    norm_gain,
    expert_ids,
    route_weight,
    gate_weight,
    up_weight,
    down_weight,
    shared_gate,
    shared_up,
    shared_down,
):
    expert_ranks = lax.axis_size("ep")
    head_ranks = lax.axis_size("tp")
    head_rank = lax.axis_index("tp")
    sequence_rows = query_rows.shape[0]
    blocks = sequence_rows // BLOCK
    pair_heads = key_rows.shape[1] // HEAD_DIM
    group_size = HEADS // KV_HEADS
    query_normed = rms_scale(
        query_rows.reshape(blocks, BLOCK, pair_heads, group_size, HEAD_DIM), query_gain
    )
    key_normed = rms_scale(key_rows.reshape(blocks, BLOCK, pair_heads, HEAD_DIM), key_gain)
    value_blocks = value_rows.reshape(blocks, BLOCK, pair_heads, HEAD_DIM)
    rim_keys, rim_values = from_behind((key_normed[blocks - 1], value_blocks[blocks - 1]), "ep", 1)
    key_band = band_blocks(rim_keys, key_normed)
    value_band = band_blocks(rim_values, value_blocks)
    window = window_mask(lax.axis_index("ep") * blocks, blocks)
    scores = (
        jnp.einsum("nqhgd,nkhd->hgnqk", query_normed, key_band, preferred_element_type=jnp.float32)
        * score_scale
    )
    scores = jnp.where(window[None, None], scores, masked_score)
    sink_col = sink_logit.reshape(pair_heads, group_size, 1, 1, 1)
    row_max = jnp.maximum(jnp.max(scores, axis=-1, keepdims=True), sink_col)
    exp_scores = jnp.exp(scores - row_max)
    attn_probs = (
        exp_scores / (jnp.sum(exp_scores, axis=-1, keepdims=True) + jnp.exp(sink_col - row_max))
    ).astype(jnp.bfloat16)
    heads_out = (
        jnp.einsum("hgnqk,nkhd->nqhgd", attn_probs, value_band, preferred_element_type=jnp.float32)
        .astype(jnp.bfloat16)
        .reshape(sequence_rows, pair_heads * group_size * HEAD_DIM)
    )
    local_experts = gate_weight.shape[0]
    expert_total = local_experts * expert_ranks
    quarter = tokens.shape[0] // head_ranks
    model_width = tokens.shape[1]
    capacity = 2 * quarter * TOP_K // expert_total
    slot_share = local_experts * capacity
    routed_rows = expert_ranks * slot_share
    normed = rms_scale(tokens, norm_gain)
    route_ids = expert_ids.reshape(head_ranks, quarter * TOP_K)
    one_hot = (route_ids[:, :, None] == jnp.arange(expert_total, dtype=jnp.int32)).astype(jnp.int32)
    slot_rank = jnp.sum(one_hot * (jnp.cumsum(one_hot, axis=1) - 1), axis=-1)
    positions = route_ids * capacity + slot_rank
    owners = jnp.arange(quarter * TOP_K, dtype=jnp.int32) // TOP_K
    padded_rows = jnp.concatenate(
        [
            normed.reshape(head_ranks, quarter, model_width),
            jnp.zeros((head_ranks, 1, model_width), jnp.bfloat16),
        ],
        axis=1,
    ).reshape(head_ranks * (quarter + 1), model_width)
    slot_token = (
        jnp.full((head_ranks, routed_rows), quarter, jnp.int32)
        .at[jnp.arange(head_ranks, dtype=jnp.int32)[:, None], positions]
        .set(jnp.broadcast_to(owners[None, :], positions.shape))
    )
    slot_index = slot_token + (jnp.arange(head_ranks, dtype=jnp.int32) * (quarter + 1))[:, None]
    own_index = lax.dynamic_index_in_dim(slot_index, head_rank, 0, keepdims=True)
    outgoing = padded_rows[own_index].reshape(1, expert_ranks, slot_share, model_width)
    arrived = lax.all_to_all(outgoing, "ep", split_axis=1, concat_axis=1, tiled=True)
    piece_rows = lax.all_gather(
        arrived.reshape(1, expert_ranks, local_experts, capacity, model_width),
        "tp",
        axis=0,
        tiled=True,
    )
    gate_part = jnp.einsum(
        "tsecd,edf->tsecf", piece_rows, gate_weight, preferred_element_type=jnp.float32
    )
    up_part = jnp.einsum(
        "tsecd,edf->tsecf", piece_rows, up_weight, preferred_element_type=jnp.float32
    )
    hidden = (jax.nn.silu(gate_part) * up_part).astype(jnp.bfloat16)
    shared_hidden = (
        jax.nn.silu(jnp.dot(normed, shared_gate, preferred_element_type=jnp.float32))
        * jnp.dot(normed, shared_up, preferred_element_type=jnp.float32)
    ).astype(jnp.bfloat16)
    span_rows = routed_rows + quarter
    mixer_out = lax.psum_scatter(
        jnp.dot(heads_out, out_weight, preferred_element_type=jnp.float32).astype(jnp.bfloat16),
        "tp",
        scatter_dimension=0,
        tiled=True,
    )
    part_count = lax.axis_size("tp") * span_rows // span_rows
    routed_part = jnp.einsum(
        "tsecf,efd->tsecd", hidden, down_weight, preferred_element_type=jnp.float32
    ).reshape(part_count, routed_rows, model_width)
    shared_part = jnp.dot(shared_hidden, shared_down, preferred_element_type=jnp.float32).reshape(
        part_count, quarter, model_width
    )
    summed = lax.psum_scatter(
        jnp.concatenate([routed_part, shared_part], axis=1)
        .reshape(part_count * span_rows, model_width)
        .astype(jnp.bfloat16),
        "tp",
        scatter_dimension=0,
        tiled=True,
    )
    returned = lax.all_to_all(
        summed[:routed_rows].reshape(expert_ranks, slot_share, model_width),
        "ep",
        split_axis=0,
        concat_axis=0,
        tiled=True,
    ).reshape(routed_rows, model_width)
    own_positions = lax.dynamic_index_in_dim(positions, head_rank, 0, keepdims=False)
    picked = returned[own_positions].reshape(quarter, TOP_K, model_width).astype(jnp.float32)
    own_weights = lax.dynamic_slice_in_dim(route_weight, head_rank * quarter, quarter, 0)
    expert_out = (
        summed[routed_rows:].astype(jnp.float32) + jnp.sum(picked * own_weights[:, :, None], axis=1)
    ).astype(jnp.bfloat16)
    return (mixer_out, expert_out)


def shards(
    query_rows,
    key_rows,
    value_rows,
    query_gain,
    key_gain,
    sink_logit,
    out_weight,
    tokens,
    norm_gain,
    expert_ids,
    route_weight,
    gate_weight,
    up_weight,
    down_weight,
    shared_gate,
    shared_up,
    shared_down,
):
    expert_ranks = lax.axis_size("ep")
    head_ranks = lax.axis_size("tp")
    head_rank = lax.axis_index("tp")
    local_experts = gate_weight.shape[0]
    expert_total = local_experts * expert_ranks
    quarter = tokens.shape[0] // head_ranks
    model_width = tokens.shape[1]
    capacity = 2 * quarter * TOP_K // expert_total
    if head_ranks != 4 or capacity % 16 or expert_ranks % 2:
        return wide_shards(
            query_rows,
            key_rows,
            value_rows,
            query_gain,
            key_gain,
            sink_logit,
            out_weight,
            tokens,
            norm_gain,
            expert_ids,
            route_weight,
            gate_weight,
            up_weight,
            down_weight,
            shared_gate,
            shared_up,
            shared_down,
        )
    slot_share = local_experts * capacity
    routed_rows = expert_ranks * slot_share
    heads_out = attention_part(query_rows, key_rows, value_rows, query_gain, key_gain, sink_logit)
    mixer_part = jnp.dot(heads_out, out_weight, preferred_element_type=jnp.float32).astype(
        jnp.bfloat16
    )
    normed = rms_scale(tokens, norm_gain)
    shared_hidden = (
        jax.nn.silu(jnp.dot(normed, shared_gate, preferred_element_type=jnp.float32))
        * jnp.dot(normed, shared_up, preferred_element_type=jnp.float32)
    ).astype(jnp.bfloat16)
    shared_part = jnp.dot(shared_hidden, shared_down, preferred_element_type=jnp.float32).astype(
        jnp.bfloat16
    )
    rank = lax.axis_index("ep")
    earlier = jnp.arange(quarter)[None, :] < jnp.arange(quarter)[:, None]
    slots = jnp.arange(routed_rows, dtype=jnp.int32)

    def slot_rows(part, count):
        own_ids = lax.dynamic_slice_in_dim(expert_ids, part * quarter, quarter, 0)
        own_normed = lax.dynamic_slice_in_dim(normed, part * quarter, quarter, 0)
        columns = [own_ids[:, i] for i in range(TOP_K)]
        positions = []
        for ids in columns:
            rank_in = sum(
                jnp.sum(((ids[:, None] == other[None, :]) & earlier).astype(jnp.int32), axis=1)
                for other in columns
            )
            owner = ids // local_experts
            half = expert_ranks // 2
            ahead = 2 * lax.rem(owner // 2 - rank // 2 + half, half) + lax.rem(owner + rank, 2)
            positions.append(
                ahead * slot_share + lax.rem(ids, local_experts) * capacity + rank_in
            )
        used = slots[: count * slot_share]
        chosen = sum((used[:, None] == spot[None, :]).astype(jnp.bfloat16) for spot in positions)
        made = jnp.dot(chosen, own_normed, preferred_element_type=jnp.float32)
        return positions, made.astype(jnp.bfloat16).reshape(count, slot_share, model_width)

    positions, outgoing = slot_rows(head_rank, expert_ranks)
    _, outgoing_peer = slot_rows(lax.rem(head_rank + 2, 4), 2)
    own_weights = lax.dynamic_slice_in_dim(route_weight, head_rank * quarter, quarter, 0)
    returned, mixer_out, shared_out = exchange(
        outgoing,
        outgoing_peer,
        mixer_part.reshape(head_ranks, quarter, model_width),
        shared_part.reshape(head_ranks, quarter, model_width),
        gate_weight,
        up_weight,
        down_weight,
        capacity,
    )
    returned = returned.reshape(routed_rows, model_width)
    routed = sum(
        jnp.dot(
            (spot[:, None] == slots[None, :]).astype(jnp.bfloat16),
            returned,
            preferred_element_type=jnp.float32,
        )
        * own_weights[:, i : i + 1]
        for i, spot in enumerate(positions)
    )
    expert_out = (shared_out.astype(jnp.float32) + routed).astype(jnp.bfloat16)
    return (mixer_out, expert_out)


def solution(mesh):
    in_specs = (
        P("ep", "tp"),
        P("ep", "tp"),
        P("ep", "tp"),
        P(),
        P(),
        P("tp"),
        P("tp", None),
        P("ep", None),
        P(),
        P("ep", None),
        P("ep", None),
        P("ep", None, "tp"),
        P("ep", None, "tp"),
        P("ep", "tp", None),
        P(None, "tp"),
        P(None, "tp"),
        P("tp", None),
    )
    out_specs = (P(("ep", "tp"), None), P(("ep", "tp"), None))
    return jax.shard_map(shards, mesh=mesh, in_specs=in_specs, out_specs=out_specs, check_vma=False)
```

profile of v0, /device:TPU:1, one launch (start us, length us, event | category | flops | bytes accessed | tf_op | source)
XLA Modules:
  0.0 173.5 jit_solution(2282164668483434530)
XLA Ops:
  0.7 0.9 slice.41
  1.5 0.7 copy.34
  2.2 4.6 %collective-permute-start = (bf16[128,2,64]{0,2,1:T(8,128)(2,1)}, bf16[128,2,64]{0,2,1:T(8,128)(2,1)}, u32[]{:S(2)}, u32[]{:S(2)}) collective-permute-start(bf16[128,2,64]{0,2,1:T(8,128)(2,1)} %bitcast.6), channel_id=1, source_target_pairs={{0,4},{4,8},{8,12},{12,16},{16,20},{20,24},{24,28},{1,5},{5,9},{9,... | collective-permute-start | bytes 98312 | tf_op jit(solution)/shard_map/ppermute | solution.py:25
  6.8 1.0 copy.38
  8.0 0.7 fusion.39
  8.8 0.6 slice_bitcast_fusion
  9.4 3.2 %collective-permute-start.1 = (bf16[128,2,64]{0,2,1:T(8,128)(2,1)}, bf16[128,2,64]{0,2,1:T(8,128)(2,1)}, u32[]{:S(2)}, u32[]{:S(2)}) collective-permute-start(bf16[128,2,64]{0,2,1:T(8,128)(2,1)} %slice_bitcast_fusion), channel_id=1, source_target_pairs={{0,4},{4,8},{8,12},{12,16},{16,20},{20,24},{24,28},{1,5},{5,9},{9,... | collective-permute-start | bytes 98312 | tf_op jit(solution)/shard_map/ppermute | solution.py:25
  12.6 2.1 %fusion = f32[512]{0:T(512)S(1)} fusion(bf16[512,2048]{1,0:T(8,128)(2,1)} %param.24), kind=kLoop, calls=%fused_computation.2 | loop fusion | flops 3145216 | bytes 2099200 | tf_op jit(solution)/shard_map/reduce_sum | solution.py:30
  14.7 0.7 constant_dynamic-slice_fusion
  15.4 0.7 constant_dynamic-slice_fusion.1
  16.1 0.2 copy.41
  16.3 0.4 reshape.481
  16.7 0.2 multiply_reduce_fusion
  17.0 0.2 convert_reduce_fusion.2
  17.2 0.2 convert_reduce_fusion.6
  17.5 0.2 broadcast_and_fusion
  17.7 1.1 multiply_convert_fusion
  18.8 2.1 %fusion.2 = bf16[512,2048]{1,0:T(8,128)(2,1)S(1)} fusion(bf16[512,2048]{1,0:T(8,128)(2,1)} %param.24, f32[2048]{0:T(1024)S(1)} %copy-done.5, f32[512]{0:T(512)S(1)} %add_rsqrt_fusion.2), kind=kLoop, calls=%fused_computation.4 | loop fusion | flops 4194304 | bytes 4204544 | tf_op jit(solution)/shard_map/convert_element_type | solution.py:31
  20.9 1.5 fusion.95
  22.5 2.1 %convolution_convert_fusion.1 = bf16[512,2048]{1,0:T(8,128)(2,1)} fusion(bf16[512,2048]{1,0:T(8,128)(2,1)S(1)} %fusion.2, s32[]{:T(128)S(6)} %select_n.91, s32[128]{0:T(128)S(1)} %get-tuple-element.32, s32[128]{0:T(128)S(1)} %get-tuple-element.33), kind=kOutput, calls=%fused_computation.11 | convolution fusion | flops 270008320 | bytes 2622468 | tf_op jit(solution)/shard_map/dot_general | solution.py:610
  24.6 1.1 convolution_convert_fusion.3
  25.7 5.0 %convolution_convert_fusion = bf16[512,2048]{1,0:T(8,128)(2,1)} fusion(bf16[256,2048]{1,0:T(8,128)(2,1)S(1)} %copy-done, bf16[512,2048]{1,0:T(8,128)(2,1)S(1)} %fusion.2, bf16[2048,256]{1,0:T(8,128)(2,1)} %param.32, f32[512,256]{1,0:T(8,128)} %fusion.95), kind=kOutput, calls=%fused_computation.10 | convolution fusion | flops 1075576832 | bytes 6815744 | tf_op jit(solution)/shard_map/dot_general | solution.py:585
  31.0 0.1 copy.36
  31.1 1.9 %fusion.4 = (f32[2,4,4,128]{3,1,2,0:T(4,128)S(1)}, f32[2,4,256,128,4]{3,2,4,1,0:T(8,128)S(1)}) fusion(pred[4,128,256]{1,2,0:T(8,128)(4,1)S(1)} %broadcast_and_fusion, bf16[4,128,2,4,64]{1,0,4,3,2:T(4,128)(2,1)} %multiply_convert_fusion, bf16[4,128,2,64]{1,3,0,2:T(8,128)(2,1)S(1)} %fusion.39, bf16[1,128,2,64]{1,3,0,2:T(8,128)(2,1)} %bitcast.11), kind=kOutput, calls=%fused_computation.9 | convolution fusion | flops 138145792 | bytes 5029888 | tf_op jit(solution)/shard_map/nqhgd,nkhd->hgnqk/dot_general | solution.py:62
  33.1 1.0 fusion.3
  34.2 2.1 %fusion.13 = bf16[4,128,2,4,64]{1,4,3,2,0:T(8,128)(2,1)S(1)} fusion(bf16[4,128,2,64]{1,3,2,0:T(8,128)(2,1)S(1)} %copy.36, bf16[1,128,2,64]{1,3,2,0:T(8,128)(2,1)} %bitcast.7, f32[2,4,256,128,4]{3,2,4,1,0:T(8,128)S(1)} %get-tuple-element.31, f32[2,4,4,128]{3,1,2,0:T(4,128)S(1)} %exponential_add_fusion, f32[2,4,4,128]{3,1,2,0:T(4,128)S(1)} %broadcast_maximum_fusion, ...), kind=kOutput, calls=%fused_computation.23 | convolution fusion | flops 140509184 | bytes 5046272 | tf_op jit(solution)/shard_map/hgnqk,nkhd->nqhgd/dot_general | solution.py:73
  36.3 0.4 copy.44
  36.7 2.6 %convolution_convert_fusion.2 = bf16[512,2048]{1,0:T(8,128)(2,1)} fusion(bf16[512,2048]{1,0:T(8,128)(2,1)S(1)} %copy-done.7, bf16[64,8,4,128]{3,2,1,0:T(4,128)(2,1)S(1)} %bitcast.93), kind=kOutput, calls=%fused_computation.12 | convolution fusion | flops 1074790400 | bytes 4718592 | tf_op jit(solution)/shard_map/dot_general | solution.py:577
  39.4 128.6 %shard_map.176 = (bf16[8,64,2048]{2,1,0:T(8,128)(2,1)}, bf16[128,2048]{1,0:T(8,128)(2,1)}, bf16[128,2048]{1,0:T(8,128)(2,1)}) custom-call(bf16[8,64,2048]{2,1,0:T(8,128)(2,1)} %bitcast.87, bf16[2,64,2048]{2,1,0:T(8,128)(2,1)} %bitcast.92, bf16[4,128,2048]{2,1,0:T(8,128)(2,1)} %bitcast.91, bf16[4,128,2048]{2,1,0:T(8,128)(2,1)} %bitcast.90, ...), custom_call_target="tpu_custom_call" | custom-call | tf_op jit(solution)/shard_map/pallas_call | solution.py:350
  168.0 2.2 %convolution_multiply_fusion.1 = f32[128,2048]{1,0:T(8,128)S(1)} fusion(bf16[512,2048]{1,0:T(8,128)(2,1)} %bitcast.88, f32[128]{0:T(128)S(1)} %get-tuple-element.21, s32[128]{0:T(128)S(1)} %get-tuple-element.19), kind=kOutput, calls=%fused_computation.16 | convolution fusion | flops 268763136 | bytes 3146752 | tf_op jit(solution)/shard_map/dot_general | solution.py:628
  170.3 2.4 %fusion.7 = bf16[128,2048]{1,0:T(8,128)(2,1)} fusion(f32[128,2048]{1,0:T(8,128)S(1)} %convolution_multiply_fusion.1, bf16[512,2048]{1,0:T(8,128)(2,1)S(1)} %bitcast.89, bf16[128,2048]{1,0:T(8,128)(2,1)} %get-tuple-element.6, f32[128]{0:T(128)S(1)} %get-tuple-element.20, s32[128]{0:T(128)S(1)} %get-tuple-element.18), kind=kOutput, calls=%fused_computation.17 | convolution fusion | flops 269811712 | bytes 4195328 | tf_op jit(solution)/shard_map/dot_general | solution.py:628
  172.7 0.8 copy.73
  (43 shorter events, 0.8 us)
Async XLA Ops:
  0.6 25.1 %copy-start = (bf16[256,2048]{1,0:T(8,128)(2,1)S(1)}, bf16[256,2048]{1,0:T(8,128)(2,1)}, u32[]{:S(2)}) copy-start(bf16[256,2048]{1,0:T(8,128)(2,1)} %param.33) | copy-start | bytes 3145732
  0.6 15.5 %copy-start.2 = (bf16[512,512]{1,0:T(8,128)(2,1)S(1)}, bf16[512,512]{1,0:T(8,128)(2,1)}, u32[]{:S(2)}) copy-start(bf16[512,512]{1,0:T(8,128)(2,1)} %param.17) | copy-start | bytes 1572868
  2.2 31.9 %collective-permute-start = (bf16[128,2,64]{0,2,1:T(8,128)(2,1)}, bf16[128,2,64]{0,2,1:T(8,128)(2,1)}, u32[]{:S(2)}, u32[]{:S(2)}) collective-permute-start(bf16[128,2,64]{0,2,1:T(8,128)(2,1)} %bitcast.6), channel_id=1, source_target_pairs={{0,4},{4,8},{8,12},{12,16},{16,20},{20,24},{24,28},{1,5},{5,9},{9,... | collective-permute-start | bytes 98312 | tf_op jit(solution)/shard_map/ppermute | solution.py:25
  7.8 9.9 %copy-start.6 = (f32[64]{0:T(128)S(1)}, f32[64]{0:T(128)}, u32[]{:S(2)}) copy-start(f32[64]{0:T(128)} %param.20) | copy-start | bytes 772
  9.4 21.7 %collective-permute-start.1 = (bf16[128,2,64]{0,2,1:T(8,128)(2,1)}, bf16[128,2,64]{0,2,1:T(8,128)(2,1)}, u32[]{:S(2)}, u32[]{:S(2)}) collective-permute-start(bf16[128,2,64]{0,2,1:T(8,128)(2,1)} %slice_bitcast_fusion), channel_id=1, source_target_pairs={{0,4},{4,8},{8,12},{12,16},{16,20},{20,24},{24,28},{1,5},{5,9},{9,... | collective-permute-start | bytes 98312 | tf_op jit(solution)/shard_map/ppermute | solution.py:25
  12.5 6.2 %copy-start.5 = (f32[2048]{0:T(1024)S(1)}, f32[2048]{0:T(1024)}, u32[]{:S(2)}) copy-start(f32[2048]{0:T(1024)} %param.25) | copy-start | bytes 24580
  16.9 4.0 %copy-start.8 = (bf16[2048,256]{1,0:T(8,128)(2,1)S(1)}, bf16[2048,256]{1,0:T(8,128)(2,1)}, u32[]{:S(2)}) copy-start(bf16[2048,256]{1,0:T(8,128)(2,1)} %param.31) | copy-start | bytes 3145732
  25.7 5.0 %copy-start.4 = (bf16[512,128]{1,0:T(8,128)(2,1)S(1)}, bf16[512,128]{1,0:T(8,128)(2,1)}, u32[]{:S(2)}) copy-start(bf16[512,128]{1,0:T(8,128)(2,1)} %param.19) | copy-start | bytes 393220
  25.7 5.1 %copy-start.9 = (f32[8]{0:T(128)S(1)}, f32[8]{0:T(128)}, u32[]{:S(2)}) copy-start(f32[8]{0:T(128)} %param.22) | copy-start | bytes 100
  34.2 2.5 %copy-start.7 = (bf16[512,2048]{1,0:T(8,128)(2,1)S(1)}, bf16[512,2048]{1,0:T(8,128)(2,1)}, u32[]{:S(2)}) copy-start(bf16[512,2048]{1,0:T(8,128)(2,1)} %param.23) | copy-start | bytes 6291460
  168.0 2.2 %copy-start.1 = (bf16[8,64,2048]{2,1,0:T(8,128)(2,1)S(1)}, bf16[8,64,2048]{2,1,0:T(8,128)(2,1)}, u32[]{:S(2)}) copy-start(bf16[8,64,2048]{2,1,0:T(8,128)(2,1)} %get-tuple-element.7) | copy-start | bytes 6291460
  168.0 4.7 %copy-start.3 = (bf16[128,2048]{1,0:T(8,128)(2,1)S(1)}, bf16[128,2048]{1,0:T(8,128)(2,1)}, u32[]{:S(2)}) copy-start(bf16[128,2048]{1,0:T(8,128)(2,1)} %get-tuple-element.36) | copy-start | bytes 1572868
where the time goes:
time: 177 us; the launch traced here: 173 us
  Pallas kernels  129 us (73%)
  matrix products  21 us (12%)
  other arithmetic  8.36 us (5%)
  starting transfers between devices  7.71 us (4%)
  local copies, waits for them, and re-layouts  6.87 us (4%)
    pallas_call x1, Pallas kernels, exchange(): pl.pallas_call(functools.partial(exchange_kernel, ranks, group, local_exp...  129 us
    ppermute x2, starting transfers between devices, from_behind(): return lax.ppermute(block, axis, route)  7.71 us
    dot_general x1, matrix products, shards(): jnp.dot(shared_hidden, shared_down, preferred_element_type=jnp.float32)  4.99 us
    dot_general x2, matrix products, shards(): jnp.dot((spot[:, None] == slots[None, :]).astype(jnp.bfloat16), returned,...  4.62 us
    convert_element_type x3, other arithmetic, rms_scale(): return (scaled * gain).astype(jnp.bfloat16)  3.96 us
  transfers between devices with their start and end apart: 2, of which 0 were waited for; matrix products, arithmetic and copies ran while one was open for 14% of the time, Pallas kernels for 0%

commit v1 on v0

v1 whole, which is shorter than its diff:
```python
import functools
import jax
import jax.numpy as jnp
from jax import lax
from jax.experimental import pallas as pl
from jax.experimental.pallas import tpu as pltpu
from jax.sharding import PartitionSpec as P

HEADS = 32
KV_HEADS = 8
HEAD_DIM = 64
WINDOW = 128
BLOCK = 128
TOP_K = 2


epsilon = 1e-06
masked_score = -1e30
score_scale = 0.125


def from_behind(block, axis, distance):
    devices = range(lax.axis_size(axis))
    route = [(i - distance, i) for i in devices if i - distance in devices]
    return lax.ppermute(block, axis, route)


def rms_scale(values, gain):
    widened = values.astype(jnp.float32)
    scaled = widened * lax.rsqrt(jnp.mean(widened * widened, axis=-1, keepdims=True) + epsilon)
    return (scaled * gain).astype(jnp.bfloat16)


def window_mask(first_block, block_count):
    query_pos = jnp.arange(BLOCK)[:, None]
    key_pos = jnp.arange(2 * BLOCK)[None, :]
    inside = (key_pos <= query_pos + BLOCK) & (key_pos > query_pos + BLOCK - WINDOW)
    not_first = (first_block + jnp.arange(block_count))[:, None, None] > 0
    return inside[None] & (not_first | (key_pos[None] >= BLOCK))


def band_blocks(rim_block, blocks_in):
    joined = jnp.concatenate([rim_block[None], blocks_in], axis=0)
    return jnp.concatenate([joined[:-1], joined[1:]], axis=1)


def layer_kernel(
    ranks,
    near,
    order,
    program,
    local_experts,
    capacity,
    sink,
    query_hbm,
    key_hbm,
    value_hbm,
    query_gain,
    key_gain,
    out_hbm,
    tokens_hbm,
    norm_gain,
    ids_hbm,
    route_hbm,
    gate_hbm,
    up_hbm,
    down_hbm,
    shared_gate_hbm,
    shared_up_hbm,
    shared_down_hbm,
    mixer_out,
    expert_out,
    rows,
    kept,
    sibling_send,
    sibling_recv,
    peer_recv,
    far_out,
    near_out,
    far_back,
    near_back,
    mixer_part,
    shared_part,
    mixer_recv,
    shared_recv,
    mixer_send,
    mixer_peer,
    merged_send,
    merged_recv,
    total,
    tok,
    query,
    key_all,
    value_all,
    key_band,
    value_band,
    heads,
    ids,
    route,
    spots,
    gate,
    up,
    down,
    out_weight,
    shared_gate,
    shared_up,
    shared_down,
    tok_sem,
    small_sem,
    weight_sem,
    rim_send,
    rim_recv,
    out_send,
    out_recv,
    fan_send,
    fan_recv,
    add_send,
    add_recv,
    back_send,
    back_recv,
    early_send,
    early_recv,
):
    rank = lax.axis_index("ep")
    part = lax.axis_index("tp")
    core = lax.rem(part, 2)
    side = part // 2
    sibling = 2 * side + 1 - core
    peer = 2 * (1 - side) + core
    across = 2 * (1 - side) + 1 - core
    placed = (part, peer, sibling, across)
    f32, bf16, i32 = jnp.float32, jnp.bfloat16, jnp.int32
    mesh_ids = pl.DeviceIdType.MESH
    width = rows.shape[-1]
    quarter = tok.shape[1]
    share = rows.shape[2]
    blocks = query.shape[0] // BLOCK
    pairs = query.shape[1] // 128
    spot_of = {k: s for s, k in enumerate(order)}
    chunk = 512
    chunks = width // chunk

    def partner(k):
        result = 0
        bit = 1
        while bit < ranks:
            own = lax.rem(rank // bit, 2)
            result = result + bit * ((1 - own) if k & bit else own)
            bit *= 2
        return result

    def send(source, target, send_sem, recv_sem, ep_to, tp_to):
        copy = pltpu.make_async_remote_copy(
            src_ref=source,
            dst_ref=target,
            send_sem=send_sem,
            recv_sem=recv_sem,
            device_id=(ep_to, tp_to),
            device_id_type=mesh_ids,
        )
        copy.start()
        sent.append(copy)
        return copy

    sent = []
    barrier = pltpu.get_barrier_semaphore()
    ahead = lax.rem(rank + 1, ranks)
    behind = lax.rem(rank + ranks - 1, ranks)
    for k in range(1, ranks):
        pl.semaphore_signal(barrier, inc=1, device_id=(partner(k), part), device_id_type=mesh_ids)
    for other in (sibling, peer):
        pl.semaphore_signal(barrier, inc=1, device_id=(rank, other), device_id_type=mesh_ids)

    def load(source, target, sem):
        copy = pltpu.make_async_copy(source, target, sem)
        copy.start()
        return copy

    def block_at(j):
        return pl.ds(pl.multiple_of(placed[j] * quarter, quarter), quarter)

    tok_loads = [load(tokens_hbm.at[block_at(j)], tok.at[j], tok_sem.at[j]) for j in range(4)]
    id_loads = [load(ids_hbm.at[block_at(j)], ids.at[j], small_sem.at[j]) for j in range(2)]
    sequence = query.shape[0]
    query_load = load(query_hbm, query, small_sem.at[4])
    key_load = load(key_hbm, key_all.at[pl.ds(BLOCK, sequence)], small_sem.at[5])
    value_load = load(value_hbm, value_all.at[pl.ds(BLOCK, sequence)], small_sem.at[6])
    weight_loads = [
        load(source, held, weight_sem.at[i])
        for i, (source, held) in enumerate(
            (
                (out_hbm, out_weight),
                (shared_gate_hbm, shared_gate),
                (shared_up_hbm, shared_up),
                (shared_down_hbm, shared_down),
                (gate_hbm, gate),
                (up_hbm, up),
                (down_hbm, down),
            )
        )
    ]
    route_loads = [load(route_hbm.at[block_at(j)], route.at[j], small_sem.at[2 + j]) for j in range(2)]

    def norm_tokens(j):
        tok_loads[j].wait()
        wide = tok[j].astype(f32)
        scaled = wide * lax.rsqrt(jnp.mean(wide * wide, axis=-1, keepdims=True) + epsilon)
        tok[j] = (scaled * norm_gain[...]).astype(bf16)

    def lay_out(j):
        id_loads[j].wait()
        lanes = lax.broadcasted_iota(i32, (quarter, 128), 1)
        below = (lanes < lax.broadcasted_iota(i32, (quarter, quarter), 0)).astype(bf16)
        columns = [ids[j][:, i : i + 1] for i in range(TOP_K)]
        hot = [(column == lanes).astype(f32) for column in columns]
        before = jnp.dot(below, sum(hot).astype(bf16), preferred_element_type=f32)
        found = []
        for i, column in enumerate(columns):
            within = jnp.sum(hot[i] * before, axis=1, keepdims=True).astype(i32)
            owner = column // local_experts
            ahead_of = 0
            bit = 1
            while bit < ranks:
                own = lax.rem(rank // bit, 2)
                theirs = lax.rem(owner // bit, 2)
                ahead_of = ahead_of + bit * (theirs + own - 2 * theirs * own)
                bit *= 2
            spot = ahead_of * share + lax.rem(column, local_experts) * capacity + within
            spots[j, :, i : i + 1] = spot
            found.append(
                jnp.transpose(jnp.broadcast_to(spot, (quarter, 128)).astype(f32))[0:1, :].astype(i32)
            )
        return found

    def slot_rows(found, j, k, count):
        used = lax.broadcasted_iota(i32, (count * share, quarter), 0) + k * share
        chosen = sum((used == spot).astype(bf16) for spot in found)
        made = jnp.dot(chosen, tok[j], preferred_element_type=f32)
        return made.astype(bf16).reshape(count, share, width)

    dispatched = {}
    to_sibling = {}
    to_peer = {}
    relayed = {}
    added = {}
    peered = {}
    backs = {}

    norm_tokens(0)
    found_own = lay_out(0)
    first_far = True
    rims = []
    for k in range(near, ranks, 2):
        count = min(2, ranks - k)
        far_out[pl.ds(k - near, count)] = slot_rows(found_own, 0, k, count)
        if first_far:
            pl.semaphore_wait(barrier, ranks + 1)
            first_far = False
        for n in range(k, k + count):
            dispatched[n] = send(
                far_out.at[n - near],
                rows.at[spot_of[n], 0],
                out_send.at[n],
                out_recv.at[n],
                partner(n),
                part,
            )
        if k == near:
            key_load.wait()
            value_load.wait()
            tail_rows = pl.ds(sequence, BLOCK)
            rims = [
                send(
                    held.at[tail_rows],
                    held.at[pl.ds(0, BLOCK)],
                    rim_send.at[i],
                    rim_recv.at[i],
                    ahead,
                    part,
                )
                for i, held in enumerate((key_all, value_all))
            ]
            norm_tokens(1)
            found_peer = lay_out(1)
            for n in range(1, near):
                near_out[n - 1, 0:1] = slot_rows(found_own, 0, n, 1)
                near_out[n - 1, 1:2] = slot_rows(found_peer, 1, n, 1)
                dispatched[n] = send(
                    near_out.at[n - 1],
                    rows.at[spot_of[n], pl.ds(0, 2)],
                    out_send.at[n],
                    out_recv.at[n],
                    partner(n),
                    part,
                )
    rows[spot_of[0], 0:1] = slot_rows(found_own, 0, 0, 1)
    rows[spot_of[0], 1:2] = slot_rows(found_peer, 1, 0, 1)

    low = lax.broadcasted_iota(i32, (BLOCK, 128), 1) < HEAD_DIM

    def head_scale(values, gain):
        squares = values * values
        lower = jnp.sum(jnp.where(low, squares, 0.0), axis=1, keepdims=True)
        upper = jnp.sum(jnp.where(low, 0.0, squares), axis=1, keepdims=True)
        mean = jnp.where(low, lower, upper) * (1.0 / HEAD_DIM)
        return values * lax.rsqrt(mean + epsilon) * gain

    def doubled(gain):
        return jnp.concatenate([gain[...], gain[...]], axis=1)

    def band_block(index, carry):
        at = pl.ds(pl.multiple_of(index * BLOCK, BLOCK), BLOCK)
        keys = head_scale(key_all[at].astype(f32), doubled(key_gain))
        values = value_all[at].astype(f32)
        for wide, band in ((keys, key_band), (values, value_band)):
            turned = pltpu.roll(wide, HEAD_DIM, 1)
            band[0, 0, at] = jnp.where(low, wide, 0.0).astype(bf16)
            band[0, 1, at] = jnp.where(low, 0.0, turned).astype(bf16)
            band[1, 0, at] = jnp.where(low, turned, 0.0).astype(bf16)
            band[1, 1, at] = jnp.where(low, 0.0, wide).astype(bf16)
        return carry

    def attend(n, slot):
        at = pl.ds(pl.multiple_of(n * BLOCK, BLOCK), BLOCK)
        span = pl.ds(pl.multiple_of(n * BLOCK, BLOCK), 2 * BLOCK)
        query_pos = lax.broadcasted_iota(i32, (BLOCK, 2 * BLOCK), 0)
        key_pos = lax.broadcasted_iota(i32, (BLOCK, 2 * BLOCK), 1)
        floor = jnp.where(rank * blocks + n > 0, 0, BLOCK)
        inside = (key_pos <= query_pos + BLOCK) & (key_pos > query_pos + BLOCK - WINDOW)
        inside = inside & (key_pos >= floor)
        for pair in range(pairs):
            kv = pair * 2 // (HEADS // KV_HEADS)
            lanes = slice(pair * 128, pair * 128 + 128)
            normed = head_scale(query[at, lanes].astype(f32), doubled(query_gain)).astype(bf16)
            keys = key_band[kv, :, span].reshape(4 * BLOCK, 128)
            scores = lax.dot_general(
                normed, keys, (((1,), (1,)), ((), ())), preferred_element_type=f32
            )
            probs = []
            for h in range(2):
                logit = sink[2 * pair + h]
                score = scores[:, h * 2 * BLOCK : (h + 1) * 2 * BLOCK] * score_scale
                score = jnp.where(inside, score, masked_score)
                top = jnp.maximum(jnp.max(score, axis=1, keepdims=True), logit)
                raised = jnp.exp(score - top)
                below = jnp.sum(raised, axis=1, keepdims=True) + jnp.exp(logit - top)
                probs.append((raised * (1.0 / below)).astype(bf16))
            values = value_band[kv, :, span].reshape(4 * BLOCK, 128)
            made = jnp.dot(jnp.concatenate(probs, axis=1), values, preferred_element_type=f32)
            heads[slot, :, lanes] = made.astype(bf16)

    def attention():
        query_load.wait()
        lax.fori_loop(1, blocks + 1, band_block, 0)
        for rim in rims:
            rim.wait_recv()
        band_block(0, 0)

        def one(j, carry):
            high = lax.rem(j, 2)
            turn = j // 2
            n = 2 * (side + high - 2 * side * high) + core + turn - 2 * core * turn
            attend(n, j)
            return carry

        lax.fori_loop(0, 4, one, 0)

    def early_pair(i, full, received):
        return send(
            full.at[pl.ds(2, 2)], received, early_send.at[i], early_recv.at[i], rank, sibling
        )

    early = {}

    def mixer():
        weight_loads[0].wait()
        for half in (1, 0):
            held = heads[2 * half : 2 * half + 2].reshape(2 * quarter, heads.shape[-1])

            def one(c, carry):
                at = pl.ds(pl.multiple_of(c * chunk, chunk), chunk)
                made = jnp.dot(held, out_weight[:, at], preferred_element_type=f32)
                mixer_part[2 * half : 2 * half + 2, :, at] = made.astype(bf16).reshape(
                    2, quarter, chunk
                )
                return carry

            lax.fori_loop(0, chunks, one, 0)
            if half:
                early["mixer"] = early_pair(0, mixer_part, mixer_recv)

    def shared():
        for i in (1, 2, 3):
            weight_loads[i].wait()
        for half in (1, 0):
            held = tok[2 * half : 2 * half + 2].reshape(2 * quarter, width)
            gate_part = jnp.dot(held, shared_gate[...], preferred_element_type=f32)
            up_part = jnp.dot(held, shared_up[...], preferred_element_type=f32)
            hidden = (gate_part / (1.0 + jnp.exp(-gate_part)) * up_part).astype(bf16)

            def one(c, carry):
                at = pl.ds(pl.multiple_of(c * chunk, chunk), chunk)
                made = jnp.dot(hidden, shared_down[:, at], preferred_element_type=f32)
                shared_part[2 * half : 2 * half + 2, :, at] = made.astype(bf16).reshape(
                    2, quarter, chunk
                )
                return carry

            lax.fori_loop(0, chunks, one, 0)
            if half:
                early["shared"] = early_pair(1, shared_part, shared_recv)

    def mixer_add():
        early["mixer"].wait_recv()
        mixer_send[...] = (mixer_part[1].astype(f32) + mixer_recv[1].astype(f32)).astype(bf16)
        early["peer"] = send(
            mixer_send, mixer_peer, early_send.at[2], early_recv.at[2], rank, peer
        )

    def mixer_finish():
        early["peer"].wait_recv()
        mixer_out[...] = (
            mixer_part[0].astype(f32) + mixer_recv[0].astype(f32) + mixer_peer[...].astype(f32)
        ).astype(bf16)

    def pass_on(k, sem, which, count):
        s = spot_of[k]
        return send(
            rows.at[s, pl.ds(which, count)],
            rows.at[s, pl.ds(2 + which, count)],
            fan_send.at[sem, k],
            fan_recv.at[sem, k],
            rank,
            sibling,
        )

    def fan(k):
        s = spot_of[k]
        if k:
            dispatched[k].wait_recv()
        if k >= near:
            to_peer[k] = send(
                rows.at[s, 0], rows.at[s, 1], fan_send.at[0, k], fan_recv.at[0, k], rank, peer
            )
            to_sibling[k] = pass_on(k, 1, 0, 1)
        else:
            to_sibling[k] = pass_on(k, 1, 0, 2)

    def relay(k):
        to_peer[k].wait_recv()
        relayed[k] = pass_on(k, 2, 1, 1)

    ready = []

    def experts(*names):
        count = len(names)
        first = spot_of[names[0]]
        for k in names:
            to_sibling[k].wait_recv()
            if k in relayed:
                relayed[k].wait_recv()
        if not ready:
            for i in (4, 5, 6):
                weight_loads[i].wait()
            ready.append(True)

        def one(index, carry):
            at = pl.ds(pl.multiple_of(index * capacity, capacity), capacity)
            block = rows[first : first + count, :, at, :].reshape(count * 4 * capacity, width)
            gate_part = jnp.dot(block, gate[index], preferred_element_type=f32)
            up_part = jnp.dot(block, up[index], preferred_element_type=f32)
            hidden = (gate_part / (1.0 + jnp.exp(-gate_part)) * up_part).astype(bf16)
            made = jnp.dot(hidden, down[index], preferred_element_type=f32)
            made = made.astype(bf16).reshape(count, 4, capacity, width)
            spot = pl.ds(first, count)
            kept[spot, :, at, :] = made[:, 0:2]
            sibling_send[spot, :, at, :] = made[:, 2:4]
            return carry

        lax.fori_loop(0, local_experts, one, 0)
        for k in names:
            s = spot_of[k]
            added[k] = send(
                sibling_send.at[s],
                sibling_recv.at[s],
                add_send.at[0, k],
                add_recv.at[0, k],
                rank,
                sibling,
            )

    def add_pair(k):
        s = spot_of[k]
        added[k].wait_recv()
        if k >= near:
            kept[s, 1] = (kept[s, 1].astype(f32) + sibling_recv[s, 1].astype(f32)).astype(bf16)
            peered[k] = send(
                kept.at[s, 1],
                peer_recv.at[k - near],
                add_send.at[1, k],
                add_recv.at[1, k],
                rank,
                peer,
            )
            return
        both = (kept[s].astype(f32) + sibling_recv[s].astype(f32)).astype(bf16)
        if k == 0:
            near_back[0] = both
            return
        kept[s] = both
        backs[k] = send(
            kept.at[s], near_back.at[k], back_send.at[k], back_recv.at[k], partner(k), part
        )

    def finish(k):
        s = spot_of[k]
        peered[k].wait_recv()
        kept[s, 0] = (
            kept[s, 0].astype(f32)
            + sibling_recv[s, 0].astype(f32)
            + peer_recv[k - near].astype(f32)
        ).astype(bf16)
        backs[k] = send(
            kept.at[s, 0], far_back.at[k - near], back_send.at[k], back_recv.at[k], partner(k), part
        )

    def picked(j, source, first):
        count = source.shape[0]
        slots = lax.broadcasted_iota(i32, (quarter, count), 1) + first
        result = 0
        for i in range(TOP_K):
            hot = (spots[j, :, i : i + 1] == slots).astype(bf16)
            result = result + jnp.dot(hot, source, preferred_element_type=f32) * route[
                j, :, i : i + 1
            ]
        return result

    def near_sum(j):
        if j:
            for k in range(1, near):
                backs[k].wait_recv()
            early["shared"].wait_recv()
            for copy in route_loads:
                copy.wait()

        def one(c, carry):
            at = pl.ds(pl.multiple_of(c * chunk, chunk), chunk)
            source = near_back[:, j, :, at].reshape(near * share, chunk)
            value = (
                shared_part[j, :, at].astype(f32)
                + shared_recv[j, :, at].astype(f32)
                + picked(j, source, 0)
            )
            if j:
                merged_send[:, at] = value.astype(bf16)
            else:
                total[:, at] = value
            return carry

        lax.fori_loop(0, chunks, one, 0)
        if j:
            early["merged"] = send(
                merged_send, merged_recv, early_send.at[3], early_recv.at[3], rank, peer
            )

    def far_sum(first, count, last):
        for k in range(first, first + count):
            backs[k].wait_recv()
        if last:
            early["merged"].wait_recv()

        def one(c, carry):
            at = pl.ds(pl.multiple_of(c * chunk, chunk), chunk)
            source = far_back[first - near : first - near + count, :, at].reshape(
                count * share, chunk
            )
            value = total[:, at] + picked(0, source, first * share)
            if last:
                value = value + merged_recv[:, at].astype(f32)
                expert_out[:, at] = value.astype(bf16)
            else:
                total[:, at] = value
            return carry

        lax.fori_loop(0, chunks, one, 0)

    steps = {
        "norm": norm_tokens,
        "attention": attention,
        "mixer": mixer,
        "shared": shared,
        "mixer_add": mixer_add,
        "mixer_finish": mixer_finish,
        "fan": fan,
        "relay": relay,
        "experts": experts,
        "add": add_pair,
        "finish": finish,
        "near_sum": near_sum,
        "far_sum": far_sum,
    }
    for name, *settings in program:
        steps[name](*settings)
    for copy in sent:
        copy.wait_send()


def step_order(ranks, near):
    half = (ranks - near) // 2
    program = [("fan", 0), ("attention",), ("fan", 4), ("fan", 1), ("norm", 2), ("norm", 3)]
    program += [("mixer",), ("relay", 4), ("shared",), ("mixer_add",), ("fan", 2)]
    program += [("experts", 0, 1), ("fan", 5), ("mixer_finish",), ("add", 0), ("add", 1)]
    program += [("relay", 5), ("experts", 4, 2), ("fan", 3), ("fan", 6)]
    program += [("add", 4), ("add", 2), ("relay", 6), ("experts", 5, 3), ("finish", 4)]
    program += [("fan", 7), ("add", 5), ("add", 3), ("relay", 7), ("finish", 5)]
    program += [("experts", 6, 7), ("add", 6), ("add", 7), ("near_sum", 1), ("near_sum", 0)]
    program += [("finish", 6), ("finish", 7), ("far_sum", 4, half, False)]
    program += [("far_sum", 4 + half, half, True)]
    return program


def layer(arrays, local_experts, capacity, ranks):
    query_rows, out_weight, tokens, gate, up, down, shared_gate, shared_up, shared_down = arrays[1]
    near = 4
    order = (0, 1, 4, 2, 5, 3, 6, 7)
    bf16, f32 = jnp.bfloat16, jnp.float32
    dma = pltpu.SemaphoreType.DMA
    quarter = tokens.shape[0] // 4
    width = tokens.shape[1]
    share = local_experts * capacity
    sequence = query_rows.shape[0]
    far = ranks - near
    vmem = pl.BlockSpec(memory_space=pltpu.VMEM)
    anywhere = pl.BlockSpec(memory_space=pl.ANY)
    smem = pl.BlockSpec(memory_space=pltpu.SMEM)

    def held(*shape):
        return pltpu.VMEM(shape, bf16)

    return pl.pallas_call(
        functools.partial(
            layer_kernel, ranks, near, order, step_order(ranks, near), local_experts, capacity
        ),
        out_shape=(
            jax.ShapeDtypeStruct((quarter, width), bf16),
            jax.ShapeDtypeStruct((quarter, width), bf16),
        ),
        in_specs=[smem]
        + [anywhere] * 3
        + [vmem] * 2
        + [anywhere] * 2
        + [vmem]
        + [anywhere] * 8,
        out_specs=(vmem, vmem),
        scratch_shapes=[
            held(ranks, 4, share, width),
            held(ranks, 2, share, width),
            held(ranks, 2, share, width),
            held(ranks, 2, share, width),
            held(far, share, width),
            held(far, share, width),
            held(near - 1, 2, share, width),
            held(far, share, width),
            held(near, 2, share, width),
            held(4, quarter, width),
            held(4, quarter, width),
            held(2, quarter, width),
            held(2, quarter, width),
            held(quarter, width),
            held(quarter, width),
            held(quarter, width),
            held(quarter, width),
            pltpu.VMEM((quarter, width), f32),
            held(4, quarter, width),
            held(*query_rows.shape),
            held(sequence + BLOCK, 128),
            held(sequence + BLOCK, 128),
            held(2, 2, sequence + BLOCK, 128),
            held(2, 2, sequence + BLOCK, 128),
            held(4, quarter, query_rows.shape[1]),
            pltpu.VMEM((2, quarter, TOP_K), jnp.int32),
            pltpu.VMEM((2, quarter, TOP_K), f32),
            pltpu.VMEM((2, quarter, TOP_K), jnp.int32),
            held(*gate.shape),
            held(*up.shape),
            held(*down.shape),
            held(*out_weight.shape),
            held(*shared_gate.shape),
            held(*shared_up.shape),
            held(*shared_down.shape),
            dma((4,)),
            dma((7,)),
            dma((7,)),
            dma((2,)),
            dma((2,)),
            dma((ranks,)),
            dma((ranks,)),
            dma((3, ranks)),
            dma((3, ranks)),
            dma((2, ranks)),
            dma((2, ranks)),
            dma((ranks,)),
            dma((ranks,)),
            dma((4,)),
            dma((4,)),
        ],
        compiler_params=pltpu.CompilerParams(
            collective_id=0, has_side_effects=True, vmem_limit_bytes=65000 * 1024
        ),
    )(*arrays[0])


def wide_shards(
    query_rows,
    key_rows,
    value_rows,
    query_gain,
    key_gain,
    sink_logit,
    out_weight,
    tokens,
    norm_gain,
    expert_ids,
    route_weight,
    gate_weight,
    up_weight,
    down_weight,
    shared_gate,
    shared_up,
    shared_down,
):
    expert_ranks = lax.axis_size("ep")
    head_ranks = lax.axis_size("tp")
    head_rank = lax.axis_index("tp")
    sequence_rows = query_rows.shape[0]
    blocks = sequence_rows // BLOCK
    pair_heads = key_rows.shape[1] // HEAD_DIM
    group_size = HEADS // KV_HEADS
    query_normed = rms_scale(
        query_rows.reshape(blocks, BLOCK, pair_heads, group_size, HEAD_DIM), query_gain
    )
    key_normed = rms_scale(key_rows.reshape(blocks, BLOCK, pair_heads, HEAD_DIM), key_gain)
    value_blocks = value_rows.reshape(blocks, BLOCK, pair_heads, HEAD_DIM)
    rim_keys, rim_values = from_behind((key_normed[blocks - 1], value_blocks[blocks - 1]), "ep", 1)
    key_band = band_blocks(rim_keys, key_normed)
    value_band = band_blocks(rim_values, value_blocks)
    window = window_mask(lax.axis_index("ep") * blocks, blocks)
    scores = (
        jnp.einsum("nqhgd,nkhd->hgnqk", query_normed, key_band, preferred_element_type=jnp.float32)
        * score_scale
    )
    scores = jnp.where(window[None, None], scores, masked_score)
    sink_col = sink_logit.reshape(pair_heads, group_size, 1, 1, 1)
    row_max = jnp.maximum(jnp.max(scores, axis=-1, keepdims=True), sink_col)
    exp_scores = jnp.exp(scores - row_max)
    attn_probs = (
        exp_scores / (jnp.sum(exp_scores, axis=-1, keepdims=True) + jnp.exp(sink_col - row_max))
    ).astype(jnp.bfloat16)
    heads_out = (
        jnp.einsum("hgnqk,nkhd->nqhgd", attn_probs, value_band, preferred_element_type=jnp.float32)
        .astype(jnp.bfloat16)
        .reshape(sequence_rows, pair_heads * group_size * HEAD_DIM)
    )
    local_experts = gate_weight.shape[0]
    expert_total = local_experts * expert_ranks
    quarter = tokens.shape[0] // head_ranks
    model_width = tokens.shape[1]
    capacity = 2 * quarter * TOP_K // expert_total
    slot_share = local_experts * capacity
    routed_rows = expert_ranks * slot_share
    normed = rms_scale(tokens, norm_gain)
    route_ids = expert_ids.reshape(head_ranks, quarter * TOP_K)
    one_hot = (route_ids[:, :, None] == jnp.arange(expert_total, dtype=jnp.int32)).astype(jnp.int32)
    slot_rank = jnp.sum(one_hot * (jnp.cumsum(one_hot, axis=1) - 1), axis=-1)
    positions = route_ids * capacity + slot_rank
    owners = jnp.arange(quarter * TOP_K, dtype=jnp.int32) // TOP_K
    padded_rows = jnp.concatenate(
        [
            normed.reshape(head_ranks, quarter, model_width),
            jnp.zeros((head_ranks, 1, model_width), jnp.bfloat16),
        ],
        axis=1,
    ).reshape(head_ranks * (quarter + 1), model_width)
    slot_token = (
        jnp.full((head_ranks, routed_rows), quarter, jnp.int32)
        .at[jnp.arange(head_ranks, dtype=jnp.int32)[:, None], positions]
        .set(jnp.broadcast_to(owners[None, :], positions.shape))
    )
    slot_index = slot_token + (jnp.arange(head_ranks, dtype=jnp.int32) * (quarter + 1))[:, None]
    own_index = lax.dynamic_index_in_dim(slot_index, head_rank, 0, keepdims=True)
    outgoing = padded_rows[own_index].reshape(1, expert_ranks, slot_share, model_width)
    arrived = lax.all_to_all(outgoing, "ep", split_axis=1, concat_axis=1, tiled=True)
    piece_rows = lax.all_gather(
        arrived.reshape(1, expert_ranks, local_experts, capacity, model_width),
        "tp",
        axis=0,
        tiled=True,
    )
    gate_part = jnp.einsum(
        "tsecd,edf->tsecf", piece_rows, gate_weight, preferred_element_type=jnp.float32
    )
    up_part = jnp.einsum(
        "tsecd,edf->tsecf", piece_rows, up_weight, preferred_element_type=jnp.float32
    )
    hidden = (jax.nn.silu(gate_part) * up_part).astype(jnp.bfloat16)
    shared_hidden = (
        jax.nn.silu(jnp.dot(normed, shared_gate, preferred_element_type=jnp.float32))
        * jnp.dot(normed, shared_up, preferred_element_type=jnp.float32)
    ).astype(jnp.bfloat16)
    span_rows = routed_rows + quarter
    mixer_out = lax.psum_scatter(
        jnp.dot(heads_out, out_weight, preferred_element_type=jnp.float32).astype(jnp.bfloat16),
        "tp",
        scatter_dimension=0,
        tiled=True,
    )
    part_count = lax.axis_size("tp") * span_rows // span_rows
    routed_part = jnp.einsum(
        "tsecf,efd->tsecd", hidden, down_weight, preferred_element_type=jnp.float32
    ).reshape(part_count, routed_rows, model_width)
    shared_part = jnp.dot(shared_hidden, shared_down, preferred_element_type=jnp.float32).reshape(
        part_count, quarter, model_width
    )
    summed = lax.psum_scatter(
        jnp.concatenate([routed_part, shared_part], axis=1)
        .reshape(part_count * span_rows, model_width)
        .astype(jnp.bfloat16),
        "tp",
        scatter_dimension=0,
        tiled=True,
    )
    returned = lax.all_to_all(
        summed[:routed_rows].reshape(expert_ranks, slot_share, model_width),
        "ep",
        split_axis=0,
        concat_axis=0,
        tiled=True,
    ).reshape(routed_rows, model_width)
    own_positions = lax.dynamic_index_in_dim(positions, head_rank, 0, keepdims=False)
    picked = returned[own_positions].reshape(quarter, TOP_K, model_width).astype(jnp.float32)
    own_weights = lax.dynamic_slice_in_dim(route_weight, head_rank * quarter, quarter, 0)
    expert_out = (
        summed[routed_rows:].astype(jnp.float32) + jnp.sum(picked * own_weights[:, :, None], axis=1)
    ).astype(jnp.bfloat16)
    return (mixer_out, expert_out)


def shards(
    query_rows,
    key_rows,
    value_rows,
    query_gain,
    key_gain,
    sink_logit,
    out_weight,
    tokens,
    norm_gain,
    expert_ids,
    route_weight,
    gate_weight,
    up_weight,
    down_weight,
    shared_gate,
    shared_up,
    shared_down,
):
    expert_ranks = lax.axis_size("ep")
    head_ranks = lax.axis_size("tp")
    local_experts = gate_weight.shape[0]
    expert_total = local_experts * expert_ranks
    quarter = tokens.shape[0] // head_ranks
    capacity = 2 * quarter * TOP_K // expert_total
    fits = (
        head_ranks == 4
        and expert_ranks == 8
        and capacity % 16 == 0
        and quarter == BLOCK
        and query_rows.shape[0] == 4 * BLOCK
        and key_rows.shape[1] == 2 * HEAD_DIM
    )
    if not fits:
        return wide_shards(
            query_rows,
            key_rows,
            value_rows,
            query_gain,
            key_gain,
            sink_logit,
            out_weight,
            tokens,
            norm_gain,
            expert_ids,
            route_weight,
            gate_weight,
            up_weight,
            down_weight,
            shared_gate,
            shared_up,
            shared_down,
        )
    operands = (
        sink_logit,
        query_rows,
        key_rows,
        value_rows,
        query_gain.reshape(1, HEAD_DIM),
        key_gain.reshape(1, HEAD_DIM),
        out_weight,
        tokens,
        norm_gain.reshape(1, tokens.shape[1]),
        expert_ids,
        route_weight,
        gate_weight,
        up_weight,
        down_weight,
        shared_gate,
        shared_up,
        shared_down,
    )
    shaped = (
        query_rows,
        out_weight,
        tokens,
        gate_weight,
        up_weight,
        down_weight,
        shared_gate,
        shared_up,
        shared_down,
    )
    return layer((operands, shaped), local_experts, capacity, expert_ranks)


def solution(mesh):
    in_specs = (
        P("ep", "tp"),
        P("ep", "tp"),
        P("ep", "tp"),
        P(),
        P(),
        P("tp"),
        P("tp", None),
        P("ep", None),
        P(),
        P("ep", None),
        P("ep", None),
        P("ep", None, "tp"),
        P("ep", None, "tp"),
        P("ep", "tp", None),
        P(None, "tp"),
        P(None, "tp"),
        P("tp", None),
    )
    out_specs = (P(("ep", "tp"), None), P(("ep", "tp"), None))
    return jax.shard_map(shards, mesh=mesh, in_specs=in_specs, out_specs=out_specs, check_vma=False)
```

time: 177 us -> 137 us (0.77); the launches traced: 173 us -> 136 us
  matrix products: 21 us -> 0 us
  other arithmetic: 8.36 us -> 0 us
  starting transfers between devices: 7.71 us -> 0 us
    dot_general x9 -> x0, matrix products: 21 us -> none  [the longest x1 4.99 us: shards(): jnp.dot(shared_hidden, shared_down, preferred_element_type=jnp.float32)]
    ppermute x2 -> x0, starting transfers between devices: 7.71 us -> none  [from_behind(): return lax.ppermute(block, axis, route)]
    unnamed x21 -> x4, local copies, waits for them, and re-layouts: 0.85 us -> 6.84 us
    convert_element_type x3 -> x0, other arithmetic: 3.96 us -> none  [rms_scale(): return (scaled * gain).astype(jnp.bfloat16)]
    reduce_sum x6 -> x0, other arithmetic: 3.8 us -> none  [the longest x3 2.37 us: rms_scale(): jnp.mean(widened * widened, axis=-1, keepdims=True) + epsilon]
    convert_element_type x5 -> x0, local copies, waits for them, and re-layouts: 2.08 us -> none  [the longest x4 1.67 us: rms_scale(): widened = values.astype(jnp.float32)]
  transfers between devices with their start and end apart: 2 -> 0, of which waited for: 0 -> 0; matrix products, arithmetic and copies ran while one was open for 14% -> 0% of each run, Pallas kernels for 0% -> 0%
where the time goes in v1:
time: 137 us; the launch traced here: 136 us
  Pallas kernels  129 us (94%)
  local copies, waits for them, and re-layouts  6.84 us (5%)
    pallas_call x1, Pallas kernels, layer(): pl.pallas_call(functools.partial(layer_kernel, ranks, near, order, step_o...  129 us
    unnamed x4, local copies, waits for them, and re-layouts  6.84 us

profile of v1, /device:TPU:1, one launch (start us, length us, event | category | flops | bytes accessed | tf_op | source)
XLA Modules:
  0.0 136.3 jit_solution(8190607075865040472)
XLA Ops:
  0.6 1.5 %copy.19.ids_hbm = s32[512,2]{1,0:T(8,128)} copy(s32[512,2]{0,1:T(2,128)} %param.26) | data formatting | bytes 8192 | tf_op args[9]
  2.2 1.5 %copy.20.route_hbm = f32[512,2]{1,0:T(8,128)} copy(f32[512,2]{0,1:T(2,128)} %param.27) | data formatting | bytes 8192 | tf_op args[10]
  3.7 128.8 %shard_map.176 = (bf16[128,2048]{1,0:T(8,128)(2,1)}, bf16[128,2048]{1,0:T(8,128)(2,1)}) custom-call(f32[8]{0:T(128)} %sink.1, bf16[512,512]{1,0:T(8,128)(2,1)} %query_hbm.1, bf16[512,128]{1,0:T(8,128)(2,1)} %key_hbm.1, bf16[512,128]{1,0:T(8,128)(2,1)} %value_hbm.1, f32[1,64]{1,0:T(1,128)} %bitcast.4, f32[1,64]{1,0:T(1,128)} %bitcast.5, ...), custom_call_target="tpu_custom_call" | custom-call | tf_op jit(solution)/shard_map/pallas_call | solution.py:640
  132.5 1.9 %copy.23 = bf16[128,2048]{1,0:T(8,128)(2,1)} copy(bf16[128,2048]{1,0:T(8,128)(2,1)} %get-tuple-element.4) | data formatting | bytes 1048576
  134.4 1.9 %copy.24 = bf16[128,2048]{1,0:T(8,128)(2,1)} copy(bf16[128,2048]{1,0:T(8,128)(2,1)} %get-tuple-element.5) | data formatting | bytes 1048576

commit v2 on v1

--- a/solution.py
+++ b/solution.py
@@ -47,6 +47,7 @@
 def layer_kernel(
     ranks,
     near,
+    direct,
     order,
     program,
     local_experts,
@@ -59,7 +60,7 @@
     key_gain,
     out_hbm,
     tokens_hbm,
-    norm_gain,
+    gain_hbm,
     ids_hbm,
     route_hbm,
     gate_hbm,
@@ -68,8 +69,7 @@
     shared_gate_hbm,
     shared_up_hbm,
     shared_down_hbm,
-    mixer_out,
-    expert_out,
+    outputs,
     rows,
     kept,
     sibling_send,
@@ -98,6 +98,10 @@
     ids,
     route,
     spots,
+    picks,
+    norm_gain,
+    far_tok,
+    far_ids,
     gate,
     up,
     down,
@@ -162,6 +166,10 @@
         sent.append(copy)
         return copy
 
+    def arrive(copy):
+        with jax.named_scope("wait"):
+            copy.wait_recv()
+
     sent = []
     barrier = pltpu.get_barrier_semaphore()
     ahead = lax.rem(rank + 1, ranks)
@@ -180,11 +188,95 @@
         return pl.ds(pl.multiple_of(placed[j] * quarter, quarter), quarter)
 
     tok_loads = [load(tokens_hbm.at[block_at(j)], tok.at[j], tok_sem.at[j]) for j in range(4)]
-    id_loads = [load(ids_hbm.at[block_at(j)], ids.at[j], small_sem.at[j]) for j in range(2)]
+    gain_load = load(gain_hbm, norm_gain, small_sem.at[0])
+    id_loads = [load(ids_hbm.at[:, block_at(j)], ids.at[j], small_sem.at[1 + j]) for j in range(2)]
     sequence = query.shape[0]
-    query_load = load(query_hbm, query, small_sem.at[4])
-    key_load = load(key_hbm, key_all.at[pl.ds(BLOCK, sequence)], small_sem.at[5])
-    value_load = load(value_hbm, value_all.at[pl.ds(BLOCK, sequence)], small_sem.at[6])
+    query_load = load(query_hbm, query, small_sem.at[5])
+    key_load = load(key_hbm, key_all.at[pl.ds(BLOCK, sequence)], small_sem.at[6])
+    value_load = load(value_hbm, value_all.at[pl.ds(BLOCK, sequence)], small_sem.at[7])
+    route_loads = [
+        load(route_hbm.at[:, block_at(j)], route.at[j], small_sem.at[3 + j]) for j in range(2)
+    ]
+
+    def norm_tokens(j):
+        scoped("load", tok_loads[j].wait)
+        wide = tok[j].astype(f32)
+        scaled = wide * lax.rsqrt(jnp.mean(wide * wide, axis=-1, keepdims=True) + epsilon)
+        tok[j] = (scaled * norm_gain[...]).astype(bf16)
+
+    def bits(value, other):
+        result = 0
+        bit = 1
+        while bit < ranks:
+            own = lax.rem(other // bit, 2)
+            theirs = lax.rem(value // bit, 2)
+            result = result + bit * (theirs + own - 2 * theirs * own)
+            bit *= 2
+        return result
+
+    def lay_out(named, source):
+        experts_all = local_experts * ranks
+        labels = lax.broadcasted_iota(i32, (experts_all, quarter), 0)
+        behind_of = lax.broadcasted_iota(i32, (quarter, quarter), 0)
+        below = (behind_of < lax.broadcasted_iota(i32, (quarter, quarter), 1)).astype(bf16)
+        lines = [named[i : i + 1, :] for i in range(TOP_K)]
+        hot = [(line == labels).astype(f32) for line in lines]
+        before = jnp.dot(sum(hot).astype(bf16), below, preferred_element_type=f32)
+        found = []
+        for i, line in enumerate(lines):
+            within = jnp.sum(hot[i] * before, axis=0, keepdims=True).astype(i32)
+            ahead_of = bits(line // local_experts, source)
+            found.append(ahead_of * share + lax.rem(line, local_experts) * capacity + within)
+        return found
+
+    def upright(line):
+        return jnp.transpose(jnp.broadcast_to(line, (quarter, quarter)))[:, 0:1]
+
+    def keep_layout(j, found):
+        for i in range(TOP_K):
+            spots[j, :, i : i + 1] = upright(found[i].astype(f32)).astype(i32)
+
+    def keep_route():
+        for j in range(2):
+            route_loads[j].wait()
+            for i in range(TOP_K):
+                picks[j, :, i : i + 1] = upright(route[j, i : i + 1, :])
+
+    def slot_rows(found, source, k, count):
+        used = lax.broadcasted_iota(i32, (count * share, quarter), 0) + k * share
+        chosen = sum((used == spot).astype(bf16) for spot in found)
+        made = jnp.dot(chosen, source[...], preferred_element_type=f32)
+        return made.astype(bf16).reshape(count, share, made.shape[1])
+
+    dispatched = {}
+    to_sibling = {}
+    to_peer = {}
+    relayed = {}
+    added = {}
+    peered = {}
+    backs = {}
+
+    def scoped(name, work, *settings):
+        with jax.named_scope(name):
+            return work(*settings)
+
+    scoped("barrier", pl.semaphore_wait, barrier, ranks + 1)
+    for copy in (key_load, value_load, *id_loads):
+        copy.wait()
+    rims = [
+        send(
+            held.at[pl.ds(sequence, BLOCK)],
+            held.at[pl.ds(0, BLOCK)],
+            rim_send.at[i],
+            rim_recv.at[i],
+            ahead,
+            part,
+        )
+        for i, held in enumerate((key_all, value_all))
+    ]
+    names_sent = send(ids.at[0], far_ids, rim_send.at[2], rim_recv.at[2], partner(near), part)
+    gain_load.wait()
+    scoped("norm_0", norm_tokens, 0)
     weight_loads = [
         load(source, held, weight_sem.at[i])
         for i, (source, held) in enumerate(
@@ -199,102 +291,88 @@
             )
         )
     ]
-    route_loads = [load(route_hbm.at[block_at(j)], route.at[j], small_sem.at[2 + j]) for j in range(2)]
-
-    def norm_tokens(j):
-        tok_loads[j].wait()
-        wide = tok[j].astype(f32)
-        scaled = wide * lax.rsqrt(jnp.mean(wide * wide, axis=-1, keepdims=True) + epsilon)
-        tok[j] = (scaled * norm_gain[...]).astype(bf16)
-
-    def lay_out(j):
-        id_loads[j].wait()
-        lanes = lax.broadcasted_iota(i32, (quarter, 128), 1)
-        below = (lanes < lax.broadcasted_iota(i32, (quarter, quarter), 0)).astype(bf16)
-        columns = [ids[j][:, i : i + 1] for i in range(TOP_K)]
-        hot = [(column == lanes).astype(f32) for column in columns]
-        before = jnp.dot(below, sum(hot).astype(bf16), preferred_element_type=f32)
-        found = []
-        for i, column in enumerate(columns):
-            within = jnp.sum(hot[i] * before, axis=1, keepdims=True).astype(i32)
-            owner = column // local_experts
-            ahead_of = 0
-            bit = 1
-            while bit < ranks:
-                own = lax.rem(rank // bit, 2)
-                theirs = lax.rem(owner // bit, 2)
-                ahead_of = ahead_of + bit * (theirs + own - 2 * theirs * own)
-                bit *= 2
-            spot = ahead_of * share + lax.rem(column, local_experts) * capacity + within
-            spots[j, :, i : i + 1] = spot
-            found.append(
-                jnp.transpose(jnp.broadcast_to(spot, (quarter, 128)).astype(f32))[0:1, :].astype(i32)
-            )
-        return found
-
-    def slot_rows(found, j, k, count):
-        used = lax.broadcasted_iota(i32, (count * share, quarter), 0) + k * share
-        chosen = sum((used == spot).astype(bf16) for spot in found)
-        made = jnp.dot(chosen, tok[j], preferred_element_type=f32)
-        return made.astype(bf16).reshape(count, share, width)
-
-    dispatched = {}
-    to_sibling = {}
-    to_peer = {}
-    relayed = {}
-    added = {}
-    peered = {}
-    backs = {}
-
-    norm_tokens(0)
-    found_own = lay_out(0)
-    first_far = True
-    rims = []
-    for k in range(near, ranks, 2):
-        count = min(2, ranks - k)
-        far_out[pl.ds(k - near, count)] = slot_rows(found_own, 0, k, count)
-        if first_far:
-            pl.semaphore_wait(barrier, ranks + 1)
-            first_far = False
-        for n in range(k, k + count):
-            dispatched[n] = send(
-                far_out.at[n - near],
-                rows.at[spot_of[n], 0],
-                out_send.at[n],
-                out_recv.at[n],
-                partner(n),
-                part,
-            )
-        if k == near:
-            key_load.wait()
-            value_load.wait()
-            tail_rows = pl.ds(sequence, BLOCK)
-            rims = [
+    found_own = scoped("lay_out_0", lay_out, ids[0], rank)
+    scoped("norm_1", norm_tokens, 1)
+    found_peer = scoped("lay_out_1", lay_out, ids[1], rank)
+
+    def give(n, source, target, h):
+        return send(
+            source,
+            target,
+            out_send.at[h, n],
+            out_recv.at[h, n],
+            partner(n if n < near else n - near),
+            part,
+        )
+
+    halves = [pl.ds(h * (width // 2), width // 2) for h in range(2)]
+    for n in range(1, near):
+        near_out[n - 1, 0:1] = scoped("near_rows", slot_rows, found_own, tok.at[0], n, 1)
+        if n < direct:
+            near_out[n - 1, 1:2] = scoped("near_rows", slot_rows, found_peer, tok.at[1], n, 1)
+            dispatched[n] = [give(n, near_out.at[n - 1], rows.at[spot_of[n], pl.ds(0, 2)], 0)]
+        else:
+            dispatched[n] = [give(n, near_out.at[n - 1, 0], rows.at[spot_of[n], 0], 0)]
+        if n == 1:
+            dense_sent = [
                 send(
-                    held.at[tail_rows],
-                    held.at[pl.ds(0, BLOCK)],
-                    rim_send.at[i],
-                    rim_recv.at[i],
-                    ahead,
+                    tok.at[0, :, columns],
+                    far_tok.at[:, columns],
+                    out_send.at[h, near],
+                    out_recv.at[h, near],
+                    partner(near),
                     part,
                 )
-                for i, held in enumerate((key_all, value_all))
+                for h, columns in enumerate(halves)
             ]
-            norm_tokens(1)
-            found_peer = lay_out(1)
-            for n in range(1, near):
-                near_out[n - 1, 0:1] = slot_rows(found_own, 0, n, 1)
-                near_out[n - 1, 1:2] = slot_rows(found_peer, 1, n, 1)
-                dispatched[n] = send(
-                    near_out.at[n - 1],
-                    rows.at[spot_of[n], pl.ds(0, 2)],
-                    out_send.at[n],
-                    out_recv.at[n],
-                    partner(n),
-                    part,
+    rows[spot_of[0], 0:1] = scoped("rows", slot_rows, found_own, tok.at[0], 0, 1)
+    rows[spot_of[0], 1:2] = scoped("rows", slot_rows, found_peer, tok.at[1], 0, 1)
+
+    def proxy(h):
+        columns = halves[h]
+        if h == 0:
+            arrive(names_sent)
+        arrive(dense_sent[h])
+        found = lay_out(far_ids[...], partner(near))
+        s = spot_of[near]
+        source = far_tok.at[:, columns]
+        rows[s, 0:1, :, columns] = slot_rows(found, source, near, 1)
+        own = rows.at[s, 0, :, columns]
+        to_peer.setdefault(near, []).append(
+            send(
+                own,
+                rows.at[s, 1, :, columns],
+                fan_send.at[3 * h, near],
+                fan_recv.at[3 * h, near],
+                rank,
+                peer,
+            )
+        )
+        to_sibling.setdefault(near, []).append(
+            send(
+                own,
+                rows.at[s, 2, :, columns],
+                fan_send.at[1 + 3 * h, near],
+                fan_recv.at[1 + 3 * h, near],
+                rank,
+                sibling,
+            )
+        )
+        for n in range(near + 1, ranks):
+            far_out[n - near - 1, :, columns] = slot_rows(found, source, n, 1)[0]
+            dispatched.setdefault(n, []).append(
+                give(
+                    n,
+                    far_out.at[n - near - 1, :, columns],
+                    rows.at[spot_of[n], 0, :, columns],
+                    h,
                 )
-    rows[spot_of[0], 0:1] = slot_rows(found_own, 0, 0, 1)
-    rows[spot_of[0], 1:2] = slot_rows(found_peer, 1, 0, 1)
+            )
+
+    def layouts():
+        keep_layout(0, found_own)
+        keep_layout(1, found_peer)
+        keep_route()
 
     low = lax.broadcasted_iota(i32, (BLOCK, 128), 1) < HEAD_DIM
 
@@ -349,21 +427,21 @@
             made = jnp.dot(jnp.concatenate(probs, axis=1), values, preferred_element_type=f32)
             heads[slot, :, lanes] = made.astype(bf16)
 
-    def attention():
+    def keys():
         query_load.wait()
         lax.fori_loop(1, blocks + 1, band_block, 0)
         for rim in rims:
-            rim.wait_recv()
+            arrive(rim)
         band_block(0, 0)
 
-        def one(j, carry):
-            high = lax.rem(j, 2)
-            turn = j // 2
-            n = 2 * (side + high - 2 * side * high) + core + turn - 2 * core * turn
+    def attend_half(half):
+        def one(step, carry):
+            j = 2 * step + half
+            n = 2 * (side + half - 2 * side * half) + core + step - 2 * core * step
             attend(n, j)
             return carry
 
-        lax.fori_loop(0, 4, one, 0)
+        lax.fori_loop(0, 2, one, 0)
 
     def early_pair(i, full, received):
         return send(
@@ -372,22 +450,27 @@
 
     early = {}
 
-    def mixer():
-        weight_loads[0].wait()
-        for half in (1, 0):
-            held = heads[2 * half : 2 * half + 2].reshape(2 * quarter, heads.shape[-1])
-
-            def one(c, carry):
-                at = pl.ds(pl.multiple_of(c * chunk, chunk), chunk)
-                made = jnp.dot(held, out_weight[:, at], preferred_element_type=f32)
-                mixer_part[2 * half : 2 * half + 2, :, at] = made.astype(bf16).reshape(
-                    2, quarter, chunk
-                )
-                return carry
-
-            lax.fori_loop(0, chunks, one, 0)
-            if half:
-                early["mixer"] = early_pair(0, mixer_part, mixer_recv)
+    def mixer(half):
+        if half:
+            weight_loads[0].wait()
+        held = jnp.concatenate([heads[half], heads[2 + half]], axis=0)
+
+        def one(c, carry):
+            at = pl.ds(pl.multiple_of(c * chunk, chunk), chunk)
+            made = jnp.dot(held, out_weight[:, at], preferred_element_type=f32).astype(bf16)
+            mixer_part[half, :, at] = made[:quarter]
+            mixer_part[2 + half, :, at] = made[quarter:]
+            return carry
+
+        lax.fori_loop(0, chunks, one, 0)
+        early["mixer", half] = send(
+            mixer_part.at[2 + half],
+            mixer_recv.at[half],
+            early_send.at[4 * half],
+            early_recv.at[4 * half],
+            rank,
+            sibling,
+        )
 
     def shared():
         for i in (1, 2, 3):
@@ -411,15 +494,16 @@
                 early["shared"] = early_pair(1, shared_part, shared_recv)
 
     def mixer_add():
-        early["mixer"].wait_recv()
+        arrive(early["mixer", 1])
         mixer_send[...] = (mixer_part[1].astype(f32) + mixer_recv[1].astype(f32)).astype(bf16)
         early["peer"] = send(
             mixer_send, mixer_peer, early_send.at[2], early_recv.at[2], rank, peer
         )
 
     def mixer_finish():
-        early["peer"].wait_recv()
-        mixer_out[...] = (
+        arrive(early["mixer", 0])
+        arrive(early["peer"])
+        outputs[0] = (
             mixer_part[0].astype(f32) + mixer_recv[0].astype(f32) + mixer_peer[...].astype(f32)
         ).astype(bf16)
 
@@ -436,18 +520,21 @@
 
     def fan(k):
         s = spot_of[k]
-        if k:
-            dispatched[k].wait_recv()
-        if k >= near:
-            to_peer[k] = send(
-                rows.at[s, 0], rows.at[s, 1], fan_send.at[0, k], fan_recv.at[0, k], rank, peer
-            )
-            to_sibling[k] = pass_on(k, 1, 0, 1)
+        for copy in dispatched.get(k, ()):
+            arrive(copy)
+        if k >= direct:
+            to_peer[k] = [
+                send(
+                    rows.at[s, 0], rows.at[s, 1], fan_send.at[0, k], fan_recv.at[0, k], rank, peer
+                )
+            ]
+            to_sibling[k] = [pass_on(k, 1, 0, 1)]
         else:
-            to_sibling[k] = pass_on(k, 1, 0, 2)
+            to_sibling[k] = [pass_on(k, 1, 0, 2)]
 
     def relay(k):
-        to_peer[k].wait_recv()
+        for copy in to_peer[k]:
+            arrive(copy)
         relayed[k] = pass_on(k, 2, 1, 1)
 
     ready = []
@@ -456,9 +543,10 @@
         count = len(names)
         first = spot_of[names[0]]
         for k in names:
-            to_sibling[k].wait_recv()
+            for copy in to_sibling[k]:
+                arrive(copy)
             if k in relayed:
-                relayed[k].wait_recv()
+                arrive(relayed[k])
         if not ready:
             for i in (4, 5, 6):
                 weight_loads[i].wait()
@@ -491,37 +579,53 @@
 
     def add_pair(k):
         s = spot_of[k]
-        added[k].wait_recv()
+        arrive(added[k])
         if k >= near:
-            kept[s, 1] = (kept[s, 1].astype(f32) + sibling_recv[s, 1].astype(f32)).astype(bf16)
-            peered[k] = send(
-                kept.at[s, 1],
-                peer_recv.at[k - near],
-                add_send.at[1, k],
-                add_recv.at[1, k],
-                rank,
-                peer,
-            )
+            for h, columns in enumerate(halves):
+                kept[s, 1, :, columns] = (
+                    kept[s, 1, :, columns].astype(f32) + sibling_recv[s, 1, :, columns].astype(f32)
+                ).astype(bf16)
+                peered[k, h] = send(
+                    kept.at[s, 1, :, columns],
+                    peer_recv.at[k - near, :, columns],
+                    add_send.at[1 + h, k],
+                    add_recv.at[1 + h, k],
+                    rank,
+                    peer,
+                )
             return
         both = (kept[s].astype(f32) + sibling_recv[s].astype(f32)).astype(bf16)
         if k == 0:
             near_back[0] = both
             return
         kept[s] = both
+
+    def give_back(k):
         backs[k] = send(
-            kept.at[s], near_back.at[k], back_send.at[k], back_recv.at[k], partner(k), part
-        )
-
-    def finish(k):
+            kept.at[spot_of[k]],
+            near_back.at[k],
+            back_send.at[0, k],
+            back_recv.at[0, k],
+            partner(k),
+            part,
+        )
+
+    def finish(k, h):
         s = spot_of[k]
-        peered[k].wait_recv()
-        kept[s, 0] = (
-            kept[s, 0].astype(f32)
-            + sibling_recv[s, 0].astype(f32)
-            + peer_recv[k - near].astype(f32)
+        columns = halves[h]
+        arrive(peered[k, h])
+        kept[s, 0, :, columns] = (
+            kept[s, 0, :, columns].astype(f32)
+            + sibling_recv[s, 0, :, columns].astype(f32)
+            + peer_recv[k - near, :, columns].astype(f32)
         ).astype(bf16)
-        backs[k] = send(
-            kept.at[s, 0], far_back.at[k - near], back_send.at[k], back_recv.at[k], partner(k), part
+        backs[k, h] = send(
+            kept.at[s, 0, :, columns],
+            far_back.at[k - near, :, columns],
+            back_send.at[h, k],
+            back_recv.at[h, k],
+            partner(k),
+            part,
         )
 
     def picked(j, source, first):
@@ -530,7 +634,7 @@
         result = 0
         for i in range(TOP_K):
             hot = (spots[j, :, i : i + 1] == slots).astype(bf16)
-            result = result + jnp.dot(hot, source, preferred_element_type=f32) * route[
+            result = result + jnp.dot(hot, source, preferred_element_type=f32) * picks[
                 j, :, i : i + 1
             ]
         return result
@@ -538,10 +642,8 @@
     def near_sum(j):
         if j:
             for k in range(1, near):
-                backs[k].wait_recv()
-            early["shared"].wait_recv()
-            for copy in route_loads:
-                copy.wait()
+                arrive(backs[k])
+            arrive(early["shared"])
 
         def one(c, carry):
             at = pl.ds(pl.multiple_of(c * chunk, chunk), chunk)
@@ -563,11 +665,13 @@
                 merged_send, merged_recv, early_send.at[3], early_recv.at[3], rank, peer
             )
 
-    def far_sum(first, count, last):
+    def far_sum(first, count):
+        last = first + count == ranks
         for k in range(first, first + count):
-            backs[k].wait_recv()
+            for h in range(2):
+                arrive(backs[k, h])
         if last:
-            early["merged"].wait_recv()
+            arrive(early["merged"])
 
         def one(c, carry):
             at = pl.ds(pl.multiple_of(c * chunk, chunk), chunk)
@@ -577,7 +681,7 @@
             value = total[:, at] + picked(0, source, first * share)
             if last:
                 value = value + merged_recv[:, at].astype(f32)
-                expert_out[:, at] = value.astype(bf16)
+                outputs[1, :, at] = value.astype(bf16)
             else:
                 total[:, at] = value
             return carry
@@ -585,8 +689,11 @@
         lax.fori_loop(0, chunks, one, 0)
 
     steps = {
+        "proxy": proxy,
+        "layouts": layouts,
         "norm": norm_tokens,
-        "attention": attention,
+        "keys": keys,
+        "attend": attend_half,
         "mixer": mixer,
         "shared": shared,
         "mixer_add": mixer_add,
@@ -595,34 +702,39 @@
         "relay": relay,
         "experts": experts,
         "add": add_pair,
+        "back": give_back,
         "finish": finish,
         "near_sum": near_sum,
         "far_sum": far_sum,
     }
     for name, *settings in program:
-        steps[name](*settings)
+        with jax.named_scope("_".join(map(str, (name, *settings)))):
+            steps[name](*settings)
     for copy in sent:
         copy.wait_send()
 
 
-def step_order(ranks, near):
-    half = (ranks - near) // 2
-    program = [("fan", 0), ("attention",), ("fan", 4), ("fan", 1), ("norm", 2), ("norm", 3)]
-    program += [("mixer",), ("relay", 4), ("shared",), ("mixer_add",), ("fan", 2)]
-    program += [("experts", 0, 1), ("fan", 5), ("mixer_finish",), ("add", 0), ("add", 1)]
-    program += [("relay", 5), ("experts", 4, 2), ("fan", 3), ("fan", 6)]
-    program += [("add", 4), ("add", 2), ("relay", 6), ("experts", 5, 3), ("finish", 4)]
-    program += [("fan", 7), ("add", 5), ("add", 3), ("relay", 7), ("finish", 5)]
-    program += [("experts", 6, 7), ("add", 6), ("add", 7), ("near_sum", 1), ("near_sum", 0)]
-    program += [("finish", 6), ("finish", 7), ("far_sum", 4, half, False)]
-    program += [("far_sum", 4 + half, half, True)]
-    return program
+def step_order(direct):
+    program = (
+        ("keys",), ("attend", 1), ("attend", 0), ("mixer", 1), ("mixer", 0), ("mixer_add",),
+        ("proxy", 0), ("proxy", 1), ("fan", 3), ("fan", 0), ("relay", 4), ("experts", 4),
+        ("fan", 5), ("fan", 2), ("relay", 3), ("experts", 2, 3), ("fan", 1), ("relay", 5),
+        ("add", 4), ("fan", 6), ("add", 3), ("back", 3), ("experts", 5), ("finish", 4, 0),
+        ("finish", 4, 1), ("add", 5), ("experts", 0, 1), ("add", 1), ("layouts",),
+        ("mixer_finish",), ("norm", 3), ("relay", 6), ("finish", 5, 0), ("finish", 5, 1),
+        ("fan", 7), ("experts", 6), ("back", 1), ("add", 2), ("back", 2), ("add", 6),
+        ("relay", 7), ("norm", 2), ("finish", 6, 0), ("finish", 6, 1), ("experts", 7),
+        ("shared",), ("add", 7), ("add", 0), ("near_sum", 1), ("finish", 7, 0),
+        ("finish", 7, 1), ("near_sum", 0), ("far_sum", 4, 2), ("far_sum", 6, 1),
+        ("far_sum", 7, 1),
+    )
+    return [step for step in program if step[0] != "relay" or step[1] >= direct]
 
 
 def layer(arrays, local_experts, capacity, ranks):
     query_rows, out_weight, tokens, gate, up, down, shared_gate, shared_up, shared_down = arrays[1]
-    near = 4
-    order = (0, 1, 4, 2, 5, 3, 6, 7)
+    near, direct = 4, 3
+    order = tuple(range(ranks))
     bf16, f32 = jnp.bfloat16, jnp.float32
     dma = pltpu.SemaphoreType.DMA
     quarter = tokens.shape[0] // 4
@@ -639,26 +751,21 @@
 
     return pl.pallas_call(
         functools.partial(
-            layer_kernel, ranks, near, order, step_order(ranks, near), local_experts, capacity
+            layer_kernel, ranks, near, direct, order, step_order(direct), local_experts, capacity
         ),
-        out_shape=(
-            jax.ShapeDtypeStruct((quarter, width), bf16),
-            jax.ShapeDtypeStruct((quarter, width), bf16),
-        ),
+        out_shape=jax.ShapeDtypeStruct((2, quarter, width), bf16),
         in_specs=[smem]
         + [anywhere] * 3
         + [vmem] * 2
-        + [anywhere] * 2
-        + [vmem]
-        + [anywhere] * 8,
-        out_specs=(vmem, vmem),
+        + [anywhere] * 11,
+        out_specs=vmem,
         scratch_shapes=[
             held(ranks, 4, share, width),
             held(ranks, 2, share, width),
             held(ranks, 2, share, width),
             held(ranks, 2, share, width),
             held(far, share, width),
-            held(far, share, width),
+            held(far - 1, share, width),
             held(near - 1, 2, share, width),
             held(far, share, width),
             held(near, 2, share, width),
@@ -678,9 +785,13 @@
             held(2, 2, sequence + BLOCK, 128),
             held(2, 2, sequence + BLOCK, 128),
             held(4, quarter, query_rows.shape[1]),
+            pltpu.VMEM((2, TOP_K, quarter), jnp.int32),
+            pltpu.VMEM((2, TOP_K, quarter), f32),
             pltpu.VMEM((2, quarter, TOP_K), jnp.int32),
             pltpu.VMEM((2, quarter, TOP_K), f32),
-            pltpu.VMEM((2, quarter, TOP_K), jnp.int32),
+            pltpu.VMEM((1, width), f32),
+            held(quarter, width),
+            pltpu.VMEM((TOP_K, quarter), jnp.int32),
             held(*gate.shape),
             held(*up.shape),
             held(*down.shape),
@@ -689,20 +800,20 @@
             held(*shared_up.shape),
             held(*shared_down.shape),
             dma((4,)),
+            dma((8,)),
             dma((7,)),
-            dma((7,)),
-            dma((2,)),
-            dma((2,)),
-            dma((ranks,)),
-            dma((ranks,)),
+            dma((3,)),
+            dma((3,)),
+            dma((2, ranks)),
+            dma((2, ranks)),
+            dma((5, ranks)),
+            dma((5, ranks)),
             dma((3, ranks)),
             dma((3, ranks)),
             dma((2, ranks)),
             dma((2, ranks)),
-            dma((ranks,)),
-            dma((ranks,)),
-            dma((4,)),
-            dma((4,)),
+            dma((5,)),
+            dma((5,)),
         ],
         compiler_params=pltpu.CompilerParams(
             collective_id=0, has_side_effects=True, vmem_limit_bytes=65000 * 1024
@@ -908,8 +1019,8 @@
         out_weight,
         tokens,
         norm_gain.reshape(1, tokens.shape[1]),
-        expert_ids,
-        route_weight,
+        expert_ids.T,
+        route_weight.T,
         gate_weight,
         up_weight,
         down_weight,
@@ -928,7 +1039,8 @@
         shared_up,
         shared_down,
     )
-    return layer((operands, shaped), local_experts, capacity, expert_ranks)
+    both = layer((operands, shaped), local_experts, capacity, expert_ranks)
+    return both[0], both[1]
 
 
 def solution(mesh):

time: 137 us -> 124 us (0.905)
  Pallas kernels: 129 us -> 120 us
  local copies, waits for them, and re-layouts: 6.84 us -> 2.28 us
    pallas_call x1, Pallas kernels: 129 us -> 120 us  [layer(): pl.pallas_call(functools.partial(layer_kernel, ranks, near, direct, order...]
    unnamed x4 -> x0, local copies, waits for them, and re-layouts: 6.84 us -> none
    squeeze x0 -> x1, local copies, waits for them, and re-layouts: none -> 2.28 us  [shards(): return (both[0], both[1])]
where the time goes in v2:
time: 124 us; the launch traced here: 122 us
  Pallas kernels  120 us (97%)
  local copies, waits for them, and re-layouts  2.28 us (2%)
    pallas_call x1, Pallas kernels, layer(): pl.pallas_call(functools.partial(layer_kernel, ranks, near, direct, order...  120 us

profile of v2, /device:TPU:1, one launch (start us, length us, event | category | flops | bytes accessed | tf_op | source)
XLA Modules:
  0.0 122.5 jit_solution(14294095001583772574)
XLA Ops:
  0.6 119.5 %shard_map.176 = bf16[2,128,2048]{2,1,0:T(8,128)(2,1)} custom-call(f32[8]{0:T(128)} %sink.1, bf16[512,512]{1,0:T(8,128)(2,1)} %query_hbm.1, bf16[512,128]{1,0:T(8,128)(2,1)} %key_hbm.1, bf16[512,128]{1,0:T(8,128)(2,1)} %value_hbm.1, f32[1,64]{1,0:T(1,128)} %bitcast.12, f32[1,64]{1,0:T(1,128)} %bitcast.13, bf16[512,2048]{1,0:T(8,128)(2,1)} %out_hbm.1, ...), custom_call_target="tpu_custom_call" | custom-call | tf_op jit(solution)/shard_map/pallas_call | solution.py:752
  120.2 2.3 %slice_bitcast_fusion = (bf16[128,2048]{1,0:T(8,128)(2,1)}, bf16[128,2048]{1,0:T(8,128)(2,1)}) fusion(bf16[2,128,2048]{2,1,0:T(8,128)(2,1)} %shard_map.176), kind=kLoop, calls=%fused_computation | loop fusion | bytes 2097152 | tf_op jit(solution)/shard_map/squeeze | solution.py:1043

commit v3 on v2

--- a/solution.py
+++ b/solution.py
@@ -70,6 +70,8 @@
     shared_up_hbm,
     shared_down_hbm,
     outputs,
+    results,
+    flush_sem,
     rows,
     kept,
     sibling_send,
@@ -246,7 +248,7 @@
         used = lax.broadcasted_iota(i32, (count * share, quarter), 0) + k * share
         chosen = sum((used == spot).astype(bf16) for spot in found)
         made = jnp.dot(chosen, source[...], preferred_element_type=f32)
-        return made.astype(bf16).reshape(count, share, made.shape[1])
+        return made.astype(bf16).reshape(count, share, width)
 
     dispatched = {}
     to_sibling = {}
@@ -295,79 +297,40 @@
     scoped("norm_1", norm_tokens, 1)
     found_peer = scoped("lay_out_1", lay_out, ids[1], rank)
 
-    def give(n, source, target, h):
-        return send(
+    def give(n, source, which, count):
+        dispatched[n] = send(
             source,
-            target,
-            out_send.at[h, n],
-            out_recv.at[h, n],
+            rows.at[spot_of[n], pl.ds(which, count)],
+            out_send.at[n],
+            out_recv.at[n],
             partner(n if n < near else n - near),
             part,
         )
 
-    halves = [pl.ds(h * (width // 2), width // 2) for h in range(2)]
     for n in range(1, near):
         near_out[n - 1, 0:1] = scoped("near_rows", slot_rows, found_own, tok.at[0], n, 1)
         if n < direct:
             near_out[n - 1, 1:2] = scoped("near_rows", slot_rows, found_peer, tok.at[1], n, 1)
-            dispatched[n] = [give(n, near_out.at[n - 1], rows.at[spot_of[n], pl.ds(0, 2)], 0)]
+            give(n, near_out.at[n - 1], 0, 2)
         else:
-            dispatched[n] = [give(n, near_out.at[n - 1, 0], rows.at[spot_of[n], 0], 0)]
+            give(n, near_out.at[n - 1, pl.ds(0, 1)], 0, 1)
         if n == 1:
-            dense_sent = [
-                send(
-                    tok.at[0, :, columns],
-                    far_tok.at[:, columns],
-                    out_send.at[h, near],
-                    out_recv.at[h, near],
-                    partner(near),
-                    part,
-                )
-                for h, columns in enumerate(halves)
-            ]
+            dense_sent = send(
+                tok.at[0], far_tok, out_send.at[0], out_recv.at[0], partner(near), part
+            )
     rows[spot_of[0], 0:1] = scoped("rows", slot_rows, found_own, tok.at[0], 0, 1)
     rows[spot_of[0], 1:2] = scoped("rows", slot_rows, found_peer, tok.at[1], 0, 1)
 
-    def proxy(h):
-        columns = halves[h]
-        if h == 0:
-            arrive(names_sent)
-        arrive(dense_sent[h])
+    def proxy():
+        arrive(names_sent)
+        arrive(dense_sent)
         found = lay_out(far_ids[...], partner(near))
         s = spot_of[near]
-        source = far_tok.at[:, columns]
-        rows[s, 0:1, :, columns] = slot_rows(found, source, near, 1)
-        own = rows.at[s, 0, :, columns]
-        to_peer.setdefault(near, []).append(
-            send(
-                own,
-                rows.at[s, 1, :, columns],
-                fan_send.at[3 * h, near],
-                fan_recv.at[3 * h, near],
-                rank,
-                peer,
-            )
-        )
-        to_sibling.setdefault(near, []).append(
-            send(
-                own,
-                rows.at[s, 2, :, columns],
-                fan_send.at[1 + 3 * h, near],
-                fan_recv.at[1 + 3 * h, near],
-                rank,
-                sibling,
-            )
-        )
-        for n in range(near + 1, ranks):
-            far_out[n - near - 1, :, columns] = slot_rows(found, source, n, 1)[0]
-            dispatched.setdefault(n, []).append(
-                give(
-                    n,
-                    far_out.at[n - near - 1, :, columns],
-                    rows.at[spot_of[n], 0, :, columns],
-                    h,
-                )
-            )
+        rows[s, 0:1] = slot_rows(found, far_tok, near, 1)
+        fan(near)
+        for n in (5, 6, 7):
+            far_out[n - near - 1] = slot_rows(found, far_tok, n, 1)[0]
+            give(n, far_out.at[pl.ds(n - near - 1, 1)], 0, 1)
 
     def layouts():
         keep_layout(0, found_own)
@@ -427,21 +390,21 @@
             made = jnp.dot(jnp.concatenate(probs, axis=1), values, preferred_element_type=f32)
             heads[slot, :, lanes] = made.astype(bf16)
 
-    def keys():
+    def attention():
         query_load.wait()
         lax.fori_loop(1, blocks + 1, band_block, 0)
         for rim in rims:
             arrive(rim)
         band_block(0, 0)
 
-    def attend_half(half):
-        def one(step, carry):
-            j = 2 * step + half
-            n = 2 * (side + half - 2 * side * half) + core + step - 2 * core * step
+        def one(j, carry):
+            high = lax.rem(j, 2)
+            turn = j // 2
+            n = 2 * (side + high - 2 * side * high) + core + turn - 2 * core * turn
             attend(n, j)
             return carry
 
-        lax.fori_loop(0, 2, one, 0)
+        lax.fori_loop(0, 4, one, 0)
 
     def early_pair(i, full, received):
         return send(
@@ -449,28 +412,24 @@
         )
 
     early = {}
-
-    def mixer(half):
-        if half:
-            weight_loads[0].wait()
-        held = jnp.concatenate([heads[half], heads[2 + half]], axis=0)
-
-        def one(c, carry):
-            at = pl.ds(pl.multiple_of(c * chunk, chunk), chunk)
-            made = jnp.dot(held, out_weight[:, at], preferred_element_type=f32).astype(bf16)
-            mixer_part[half, :, at] = made[:quarter]
-            mixer_part[2 + half, :, at] = made[quarter:]
-            return carry
-
-        lax.fori_loop(0, chunks, one, 0)
-        early["mixer", half] = send(
-            mixer_part.at[2 + half],
-            mixer_recv.at[half],
-            early_send.at[4 * half],
-            early_recv.at[4 * half],
-            rank,
-            sibling,
-        )
+    flushes = []
+
+    def mixer():
+        weight_loads[0].wait()
+        for half in (1, 0):
+            held = heads[2 * half : 2 * half + 2].reshape(2 * quarter, heads.shape[-1])
+
+            def one(c, carry):
+                at = pl.ds(pl.multiple_of(c * chunk, chunk), chunk)
+                made = jnp.dot(held, out_weight[:, at], preferred_element_type=f32)
+                mixer_part[2 * half : 2 * half + 2, :, at] = made.astype(bf16).reshape(
+                    2, quarter, chunk
+                )
+                return carry
+
+            lax.fori_loop(0, chunks, one, 0)
+            if half:
+                early["mixer"] = early_pair(0, mixer_part, mixer_recv)
 
     def shared():
         for i in (1, 2, 3):
@@ -494,18 +453,18 @@
                 early["shared"] = early_pair(1, shared_part, shared_recv)
 
     def mixer_add():
-        arrive(early["mixer", 1])
+        arrive(early["mixer"])
         mixer_send[...] = (mixer_part[1].astype(f32) + mixer_recv[1].astype(f32)).astype(bf16)
         early["peer"] = send(
             mixer_send, mixer_peer, early_send.at[2], early_recv.at[2], rank, peer
         )
 
     def mixer_finish():
-        arrive(early["mixer", 0])
         arrive(early["peer"])
-        outputs[0] = (
+        results[0] = (
             mixer_part[0].astype(f32) + mixer_recv[0].astype(f32) + mixer_peer[...].astype(f32)
         ).astype(bf16)
+        flushes.append(load(results.at[0], outputs.at[0], flush_sem.at[chunks]))
 
     def pass_on(k, sem, which, count):
         s = spot_of[k]
@@ -520,21 +479,18 @@
 
     def fan(k):
         s = spot_of[k]
-        for copy in dispatched.get(k, ()):
-            arrive(copy)
+        if k not in (0, near):
+            arrive(dispatched[k])
         if k >= direct:
-            to_peer[k] = [
-                send(
-                    rows.at[s, 0], rows.at[s, 1], fan_send.at[0, k], fan_recv.at[0, k], rank, peer
-                )
-            ]
-            to_sibling[k] = [pass_on(k, 1, 0, 1)]
+            to_peer[k] = send(
+                rows.at[s, 0], rows.at[s, 1], fan_send.at[0, k], fan_recv.at[0, k], rank, peer
+            )
+            to_sibling[k] = pass_on(k, 1, 0, 1)
         else:
-            to_sibling[k] = [pass_on(k, 1, 0, 2)]
+            to_sibling[k] = pass_on(k, 1, 0, 2)
 
     def relay(k):
-        for copy in to_peer[k]:
-            arrive(copy)
+        arrive(to_peer[k])
         relayed[k] = pass_on(k, 2, 1, 1)
 
     ready = []
@@ -543,8 +499,7 @@
         count = len(names)
         first = spot_of[names[0]]
         for k in names:
-            for copy in to_sibling[k]:
-                arrive(copy)
+            arrive(to_sibling[k])
             if k in relayed:
                 arrive(relayed[k])
         if not ready:
@@ -581,18 +536,15 @@
         s = spot_of[k]
         arrive(added[k])
         if k >= near:
-            for h, columns in enumerate(halves):
-                kept[s, 1, :, columns] = (
-                    kept[s, 1, :, columns].astype(f32) + sibling_recv[s, 1, :, columns].astype(f32)
-                ).astype(bf16)
-                peered[k, h] = send(
-                    kept.at[s, 1, :, columns],
-                    peer_recv.at[k - near, :, columns],
-                    add_send.at[1 + h, k],
-                    add_recv.at[1 + h, k],
-                    rank,
-                    peer,
-                )
+            kept[s, 1] = (kept[s, 1].astype(f32) + sibling_recv[s, 1].astype(f32)).astype(bf16)
+            peered[k] = send(
+                kept.at[s, 1],
+                peer_recv.at[k - near],
+                add_send.at[1, k],
+                add_recv.at[1, k],
+                rank,
+                peer,
+            )
             return
         both = (kept[s].astype(f32) + sibling_recv[s].astype(f32)).astype(bf16)
         if k == 0:
@@ -604,28 +556,22 @@
         backs[k] = send(
             kept.at[spot_of[k]],
             near_back.at[k],
-            back_send.at[0, k],
-            back_recv.at[0, k],
+            back_send.at[k],
+            back_recv.at[k],
             partner(k),
             part,
         )
 
-    def finish(k, h):
+    def finish(k):
         s = spot_of[k]
-        columns = halves[h]
-        arrive(peered[k, h])
-        kept[s, 0, :, columns] = (
-            kept[s, 0, :, columns].astype(f32)
-            + sibling_recv[s, 0, :, columns].astype(f32)
-            + peer_recv[k - near, :, columns].astype(f32)
+        arrive(peered[k])
+        kept[s, 0] = (
+            kept[s, 0].astype(f32)
+            + sibling_recv[s, 0].astype(f32)
+            + peer_recv[k - near].astype(f32)
         ).astype(bf16)
-        backs[k, h] = send(
-            kept.at[s, 0, :, columns],
-            far_back.at[k - near, :, columns],
-            back_send.at[h, k],
-            back_recv.at[h, k],
-            partner(k),
-            part,
+        backs[k] = send(
+            kept.at[s, 0], far_back.at[k - near], back_send.at[k], back_recv.at[k], partner(k), part
         )
 
     def picked(j, source, first):
@@ -668,8 +614,7 @@
     def far_sum(first, count):
         last = first + count == ranks
         for k in range(first, first + count):
-            for h in range(2):
-                arrive(backs[k, h])
+            arrive(backs[k])
         if last:
             arrive(early["merged"])
 
@@ -681,19 +626,26 @@
             value = total[:, at] + picked(0, source, first * share)
             if last:
                 value = value + merged_recv[:, at].astype(f32)
-                outputs[1, :, at] = value.astype(bf16)
+                results[1, :, at] = value.astype(bf16)
             else:
                 total[:, at] = value
             return carry
 
-        lax.fori_loop(0, chunks, one, 0)
+        if last:
+            for c in range(chunks):
+                one(c, 0)
+                at = pl.ds(c * chunk, chunk)
+                flushes.append(
+                    load(results.at[1, :, at], outputs.at[1, :, at], flush_sem.at[c])
+                )
+        else:
+            lax.fori_loop(0, chunks, one, 0)
 
     steps = {
         "proxy": proxy,
         "layouts": layouts,
         "norm": norm_tokens,
-        "keys": keys,
-        "attend": attend_half,
+        "attention": attention,
         "mixer": mixer,
         "shared": shared,
         "mixer_add": mixer_add,
@@ -712,20 +664,20 @@
             steps[name](*settings)
     for copy in sent:
         copy.wait_send()
+    for copy in flushes:
+        copy.wait()
 
 
 def step_order(direct):
     program = (
-        ("keys",), ("attend", 1), ("attend", 0), ("mixer", 1), ("mixer", 0), ("mixer_add",),
-        ("proxy", 0), ("proxy", 1), ("fan", 3), ("fan", 0), ("relay", 4), ("experts", 4),
-        ("fan", 5), ("fan", 2), ("relay", 3), ("experts", 2, 3), ("fan", 1), ("relay", 5),
-        ("add", 4), ("fan", 6), ("add", 3), ("back", 3), ("experts", 5), ("finish", 4, 0),
-        ("finish", 4, 1), ("add", 5), ("experts", 0, 1), ("add", 1), ("layouts",),
-        ("mixer_finish",), ("norm", 3), ("relay", 6), ("finish", 5, 0), ("finish", 5, 1),
-        ("fan", 7), ("experts", 6), ("back", 1), ("add", 2), ("back", 2), ("add", 6),
-        ("relay", 7), ("norm", 2), ("finish", 6, 0), ("finish", 6, 1), ("experts", 7),
-        ("shared",), ("add", 7), ("add", 0), ("near_sum", 1), ("finish", 7, 0),
-        ("finish", 7, 1), ("near_sum", 0), ("far_sum", 4, 2), ("far_sum", 6, 1),
+        ("fan", 0), ("attention",), ("fan", 1), ("fan", 2), ("fan", 3), ("proxy",),
+        ("experts", 0, 1), ("relay", 2), ("add", 0), ("relay", 3), ("fan", 5),
+        ("experts", 2, 3), ("relay", 4), ("fan", 6), ("add", 3), ("back", 3), ("relay", 5),
+        ("add", 2), ("fan", 7), ("experts", 4), ("experts", 5), ("norm", 2), ("add", 1),
+        ("mixer",), ("add", 5), ("norm", 3), ("back", 2), ("back", 1), ("add", 4), ("shared",),
+        ("relay", 6), ("finish", 5), ("layouts",), ("mixer_add",), ("relay", 7), ("finish", 4),
+        ("experts", 6, 7), ("add", 6), ("add", 7), ("near_sum", 1), ("mixer_finish",),
+        ("finish", 6), ("near_sum", 0), ("finish", 7), ("far_sum", 6, 1), ("far_sum", 4, 2),
         ("far_sum", 7, 1),
     )
     return [step for step in program if step[0] != "relay" or step[1] >= direct]
@@ -733,7 +685,7 @@
 
 def layer(arrays, local_experts, capacity, ranks):
     query_rows, out_weight, tokens, gate, up, down, shared_gate, shared_up, shared_down = arrays[1]
-    near, direct = 4, 3
+    near, direct = 4, 2
     order = tuple(range(ranks))
     bf16, f32 = jnp.bfloat16, jnp.float32
     dma = pltpu.SemaphoreType.DMA
@@ -758,8 +710,10 @@
         + [anywhere] * 3
         + [vmem] * 2
         + [anywhere] * 11,
-        out_specs=vmem,
+        out_specs=anywhere,
         scratch_shapes=[
+            held(2, quarter, width),
+            dma((width // 512 + 1,)),
             held(ranks, 4, share, width),
             held(ranks, 2, share, width),
             held(ranks, 2, share, width),
@@ -804,16 +758,16 @@
             dma((7,)),
             dma((3,)),
             dma((3,)),
-            dma((2, ranks)),
-            dma((2, ranks)),
-            dma((5, ranks)),
-            dma((5, ranks)),
+            dma((ranks,)),
+            dma((ranks,)),
             dma((3, ranks)),
             dma((3, ranks)),
             dma((2, ranks)),
             dma((2, ranks)),
-            dma((5,)),
-            dma((5,)),
+            dma((ranks,)),
+            dma((ranks,)),
+            dma((4,)),
+            dma((4,)),
         ],
         compiler_params=pltpu.CompilerParams(
             collective_id=0, has_side_effects=True, vmem_limit_bytes=65000 * 1024

time: 124 us -> 118 us (0.952)
  the two profiles are of different devices: /device:TPU:1 before, /device:TPU:8 now
where the time goes in v3:
time: 118 us
  Pallas kernels  115 us (97%)
  local copies, waits for them, and re-layouts  2.28 us (2%)
    pallas_call x1, Pallas kernels, layer(): pl.pallas_call(functools.partial(layer_kernel, ranks, near, direct, order...  115 us

profile of v3, /device:TPU:8, one launch (start us, length us, event | category | flops | bytes accessed | tf_op | source)
XLA Modules:
  0.0 118.0 jit_solution(6298976563090083496)
XLA Ops:
  0.6 115.1 %shard_map.176 = bf16[2,128,2048]{2,1,0:T(8,128)(2,1)} custom-call(f32[8]{0:T(128)} %sink.1, bf16[512,512]{1,0:T(8,128)(2,1)} %query_hbm.1, bf16[512,128]{1,0:T(8,128)(2,1)} %key_hbm.1, bf16[512,128]{1,0:T(8,128)(2,1)} %value_hbm.1, f32[1,64]{1,0:T(1,128)} %bitcast.12, f32[1,64]{1,0:T(1,128)} %bitcast.13, bf16[512,2048]{1,0:T(8,128)(2,1)} %out_hbm.1, ...), custom_call_target="tpu_custom_call" | custom-call | tf_op jit(solution)/shard_map/pallas_call | solution.py:704
  115.8 2.3 %slice_bitcast_fusion = (bf16[128,2048]{1,0:T(8,128)(2,1)}, bf16[128,2048]{1,0:T(8,128)(2,1)}) fusion(bf16[2,128,2048]{2,1,0:T(8,128)(2,1)} %shard_map.176), kind=kLoop, calls=%fused_computation | loop fusion | bytes 2097152 | tf_op jit(solution)/shard_map/squeeze | solution.py:997
